TPU v7x, 256 devices: a whole 4x4x8 slice. The times are simulated.
256 devices in a mesh: dp: 4 (over y), kv: 32 (over z, x), tp: 2 (over core).
Axes of the slice: x: 4, y: 4, z: 8, core: 2. Of those that a mesh axis runs over, the one named last changes fastest.
Arguments:
- tokens: bfloat16 [16, 16, 2048], P('dp', None, 'kv'), may hold values from -6 to 6
- norm_gain: float32 [2048], P('kv'), may hold values from 0.1 to 1.9
- w_query: bfloat16 [2048, 1024], P('kv', 'tp'), may hold values from -0.125 to 0.125
- w_key: bfloat16 [2048, 1024], P('kv', 'tp'), may hold values from -0.125 to 0.125
- w_value: bfloat16 [2048, 1024], P('kv', 'tp'), may hold values from -0.125 to 0.125
- w_forget: bfloat16 [2048, 16], replicated, may hold values from -0.125 to 0.125
- forget_bias: float32 [16], replicated, may hold values from -2 to 4
- query_gain: float32 [64], replicated, may hold values from 0.1 to 1.9
- key_gain: float32 [64], replicated, may hold values from 0.1 to 1.9
- head_gain: float32 [64], replicated, may hold values from 0.1 to 1.9
- w_out: bfloat16 [1024, 2048], P('tp', 'kv'), may hold values from -0.1875 to 0.1875
- key_cache: bfloat16 [16, 16384, 1024], P('dp', 'kv', 'tp'), may hold values from -240 to 240
- value_cache: bfloat16 [16, 16384, 1024], P('dp', 'kv', 'tp'), may hold values from -6 to 6
- gate_cache: float32 [16, 16, 16384], P('dp', 'tp', 'kv'), may hold values from -1922 to 0, as said below
- lengths: int32 [16], P('dp'), may hold values from 15341 to 16364
- accepted: int32 [16], P('dp'), may hold values from 0 to 4
- parents: int32 [16, 16], P('dp'), may hold values from -1 to 14, as said below
Outputs:
- layer_out: bfloat16 [16, 16, 2048], P('dp', None, 'kv')
- new_keys: bfloat16 [16, 16384, 1024], P('dp', 'kv', 'tp')
- new_values: bfloat16 [16, 16384, 1024], P('dp', 'kv', 'tp')
- proposal_gates: float32 [16, 16, 16], P('dp', None, 'tp')
Inputs may be any that keep to these rules, and one draw needn't show every extreme that they name: `gate_cache`: each entry is the running sum of log forget gates up to its position, so entries never rise along positions; entries at and after lengths hold the last step's proposals in order. `parents`: proposal 0 follows the last accepted token (parent -1); every other proposal's parent is one of the three proposals before it.
All inputs are finite; a program needn't handle non-finite values.
Results may differ from a plain program's by a relative error of at most 0.0051.
The roundings to bfloat16 on the way count: a program that leaves them out, or rounds other values in their place, can miss the bound.
Values may be sent and summed in bfloat16 or wider, within the bound.
No kernel may reach another device: no remote copies, remote signals or barrier semaphores. Data moves between devices by JAX's collectives and lax.ppermute only.
A program may use at most 64 MiB of HBM per device.

v0:
```python
import jax
import jax.numpy as jnp
from jax import lax
from jax.sharding import PartitionSpec as P

EPSILON = 1e-06
MASKED = -1e30


def padded_to(lines, devices):
    spare = -lines.shape[0] % devices
    if not spare:
        return lines
    return jnp.concatenate([lines, jnp.zeros((spare, *lines.shape[1:]), lines.dtype)])


def from_everyone(array, axis):
    devices = lax.axis_size(axis)
    return lax.all_to_all(
        jnp.broadcast_to(array[None], (devices, *array.shape)), axis, 0, 0, tiled=True
    )


def joined_along(parts, dim):
    parts = jnp.moveaxis(parts, 0, dim)
    lengths = parts.shape
    return parts.reshape(*lengths[:dim], lengths[dim] * lengths[dim + 1], *lengths[dim + 2 :])


def collect(array, axis, dim):
    parts = from_everyone(array, axis)
    return joined_along(parts, dim)


def cut_along(array, dim, devices):
    before, after = (array.shape[:dim], array.shape[dim + 1 :])
    return jnp.moveaxis(array.reshape(*before, devices, -1, *after), dim, 0)


def summed_on_arrival(array, axis, dim):
    parts = cut_along(array, dim, lax.axis_size(axis))
    arrived = lax.all_to_all(parts, axis, split_axis=0, concat_axis=0, tiled=True)
    return arrived.sum(axis=0)


def total_of(array, axes):
    padded = padded_to(array, lax.axis_size(axes))
    whole = collect(summed_on_arrival(padded, axes, 0), axes, 0)
    return lax.slice_in_dim(whole, 0, len(array)).reshape(array.shape)


def packed_total(arrays, axis):
    ends = [0]
    for a in arrays:
        ends.append(ends[-1] + a.size)
    total = total_of(jnp.concatenate([a.ravel() for a in arrays]), axis)
    return tuple((total[b:e].reshape(a.shape) for a, b, e in zip(arrays, ends, ends[1:])))


def of_everyone(array, axis):
    return from_everyone(array, axis).astype(jnp.float32).sum(axis=0)


def head_norm(head_rows, gain_vec):
    mean_square = jnp.mean(head_rows * head_rows, axis=-1, keepdims=True)
    return head_rows * lax.rsqrt(mean_square + EPSILON) * gain_vec


def ancestry(parents):
    count_all = parents.shape[1]
    step_ids = jnp.arange(count_all, dtype=jnp.int32)
    step_matrix = (parents[:, :, None] == step_ids[None, None, :]).astype(jnp.float32)
    identity = jnp.broadcast_to(jnp.eye(count_all, dtype=jnp.float32), step_matrix.shape)

    def extend(turn_index, ancestors):
        return identity + jnp.einsum(
            "sij,sjk->sik", step_matrix, ancestors, precision=lax.Precision.HIGHEST
        )

    return lax.fori_loop(0, count_all, extend, identity)


def combine(earlier, later):
    earlier_max, earlier_total, earlier_sum = earlier
    later_max, later_total, later_sum = later
    row_max = jnp.maximum(earlier_max, later_max)
    earlier_scale = jnp.exp(earlier_max - row_max)
    later_scale = jnp.exp(later_max - row_max)
    spread = earlier_max.shape + (-1,)
    joined = (
        earlier_sum.reshape(spread) * earlier_scale[..., None]
        + later_sum.reshape(spread) * later_scale[..., None]
    )
    return (
        row_max,
        earlier_total * earlier_scale + later_total * later_scale,
        joined.reshape(earlier_sum.shape),
    )


def block_part(scores, live_mask, block_values):
    seq_count, heads_local, prop_count, key_count = scores.shape
    row_max = jnp.max(scores, axis=3)
    weights = jnp.where(live_mask, jnp.exp(scores - row_max[..., None]), 0.0)
    row_total = jnp.sum(weights, axis=3)
    weighted = jnp.einsum(
        "shpk,skhd->sphd",
        weights.astype(jnp.bfloat16),
        block_values,
        preferred_element_type=jnp.float32,
    )
    return (
        jnp.transpose(row_max, (0, 2, 1)),
        jnp.transpose(row_total, (0, 2, 1)),
        weighted.reshape(seq_count, prop_count, -1),
    )


def finish_rows(row_sums, inverse, query_gain, key_gain, heads_local):
    head_width = row_sums.shape[1] // 3
    head_size = head_width // heads_local
    row_count = row_sums.shape[0]
    raw_sums = row_sums * inverse[:, None]
    queries = head_norm(
        raw_sums[:, :head_width].reshape(row_count, heads_local, head_size), query_gain
    )
    keyed = head_norm(
        raw_sums[:, head_width : 2 * head_width].reshape(row_count, heads_local, head_size),
        key_gain,
    )
    return jnp.concatenate(
        [
            queries.reshape(row_count, head_width),
            keyed.reshape(row_count, head_width),
            raw_sums[:, 2 * head_width :],
        ],
        axis=1,
    ).astype(jnp.bfloat16)


def flatten_part(part_triple, rows_all):
    part_max, part_total, part_sum = part_triple
    return (
        part_max.reshape(rows_all, -1),
        part_total.reshape(rows_all, -1),
        part_sum.reshape(rows_all, -1),
    )


def shards(
    tokens,
    norm_gain,
    w_query,
    w_key,
    w_value,
    w_forget,
    forget_bias,
    query_gain,
    key_gain,
    head_gain,
    w_out,
    key_cache,
    value_cache,
    gate_cache,
    lengths,
    accepted,
    parents,
):
    seq_count, prop_count, width_in = tokens.shape
    pos_dev = key_cache.shape[1]
    heads_local = gate_cache.shape[1]
    head_width = key_cache.shape[2]
    head_size = head_width // heads_local
    rows_all = seq_count * prop_count
    full_width = w_forget.shape[0]
    kv_index = lax.axis_index("kv")
    tp_index = lax.axis_index("tp")
    flattened = tokens.reshape(rows_all, width_in).astype(jnp.float32)
    squares = jnp.sum(flattened * flattened, axis=1)
    scaled = (flattened * norm_gain).astype(jnp.bfloat16)
    w_rows = lax.dynamic_slice_in_dim(w_forget, kv_index * width_in, width_in, 0)
    gate_part = jnp.dot(scaled, w_rows, preferred_element_type=jnp.float32)
    w_joined = jnp.concatenate([w_query, w_key, w_value], axis=1)
    summed, gate_sum, square_sum = packed_total(
        (jnp.dot(scaled, w_joined, preferred_element_type=jnp.float32), gate_part, squares), "kv"
    )
    inverse = lax.rsqrt(square_sum / full_width + EPSILON)
    joined = finish_rows(summed, inverse, query_gain, key_gain, heads_local)
    log_all = jax.nn.log_sigmoid(gate_sum * inverse[:, None] + forget_bias)
    log_own = lax.dynamic_slice_in_dim(log_all, tp_index * heads_local, heads_local, 1)
    log_own = log_own.reshape(seq_count, prop_count, heads_local)
    queries = joined[:, :head_width].reshape(seq_count, prop_count, heads_local, head_size)
    keys_new = joined[:, head_width : 2 * head_width].reshape(
        seq_count, prop_count, heads_local, head_size
    )
    values_new = joined[:, 2 * head_width :].reshape(seq_count, prop_count, heads_local, head_size)
    ancestors = ancestry(parents)
    path_sum = jnp.einsum("sij,sjh->sih", ancestors, log_own, precision=lax.Precision.HIGHEST)
    base_pos = lengths + accepted
    positions = kv_index * pos_dev + jnp.arange(pos_dev, dtype=jnp.int32)
    score_scale = head_size ** (-0.5)
    cached_keys = key_cache.reshape(seq_count, pos_dev, heads_local, head_size)
    cached_values = value_cache.reshape(seq_count, pos_dev, heads_local, head_size)
    scores = jnp.einsum("sphd,skhd->shpk", queries, cached_keys, preferred_element_type=jnp.float32)
    scores = scores * score_scale - gate_cache[:, :, None, :]
    live_mask = (positions[None, :] < base_pos[:, None])[:, None, None, :]
    scores = jnp.where(live_mask, scores, MASKED)
    local_part = block_part(scores, live_mask, cached_values)
    hit_mask = positions[None, :] == (base_pos - 1)[:, None]
    boundary_local = jnp.sum(jnp.where(hit_mask[:, None, :], gate_cache, 0.0), axis=2)
    tree_live = (ancestors > 0.5)[:, None, :, :]
    owner_mask = jnp.any(hit_mask, axis=1)
    tree_scores = jnp.einsum(
        "sphd,sjhd->shpj", queries, keys_new, preferred_element_type=jnp.float32
    )
    tree_scores = (
        tree_scores * score_scale
        - jnp.transpose(path_sum, (0, 2, 1))[:, :, None, :]
        - boundary_local[:, :, None, None]
    )
    tree_scores = jnp.where(tree_live, tree_scores, MASKED)
    tree_max, tree_total, tree_sum = block_part(tree_scores, tree_live, values_new)
    tree_max = jnp.where(owner_mask[:, None, None], tree_max, MASKED)
    tree_total = jnp.where(owner_mask[:, None, None], tree_total, 0.0)
    tree_sum = jnp.where(owner_mask[:, None, None], tree_sum, 0.0)
    partial_value = combine(local_part, (tree_max, tree_total, tree_sum))
    flat_max, flat_total, flat_sum = flatten_part(partial_value, rows_all)
    got_max, got_total, got_sum = (
        lax.all_to_all(flat_max[None], "kv", split_axis=1, concat_axis=0, tiled=True),
        lax.all_to_all(flat_total[None], "kv", split_axis=1, concat_axis=0, tiled=True),
        lax.all_to_all(flat_sum[None], "kv", split_axis=1, concat_axis=0, tiled=True),
    )
    top = jnp.max(got_max, axis=0)
    factors = jnp.exp(got_max - top[None])
    own_rows = got_max.shape[1]
    summed_rows = jnp.sum(
        got_sum.reshape(got_sum.shape[0], own_rows, heads_local, head_size) * factors[..., None],
        axis=0,
    )
    merged = (top, jnp.sum(got_total * factors, axis=0), summed_rows.reshape(own_rows, head_width))
    row_max, row_total, weighted = merged
    attended = weighted.reshape(own_rows, heads_local, head_size) / row_total[..., None]
    own_normed = head_norm(attended, head_gain).astype(jnp.bfloat16).reshape(own_rows, head_width)
    normed = collect(own_normed, "kv", 0)
    out_term = jnp.dot(normed, w_out, preferred_element_type=jnp.float32)
    layer_out = (
        of_everyone(out_term.astype(jnp.bfloat16), "tp").astype(jnp.float32).astype(jnp.bfloat16)
    )
    layer_out = layer_out.reshape(seq_count, prop_count, -1)
    new_rows = jnp.concatenate(
        [
            keys_new.reshape(seq_count, prop_count, head_width),
            values_new.reshape(seq_count, prop_count, head_width),
        ],
        axis=2,
    )
    slot_index = positions[None, :, None] - base_pos[:, None, None]
    placing = slot_index == jnp.arange(prop_count, dtype=jnp.int32)[None, None, :]
    written = jnp.einsum(
        "skp,spc->skc", placing.astype(jnp.bfloat16), new_rows, preferred_element_type=jnp.float32
    ).astype(jnp.bfloat16)
    hit_rows = jnp.any(placing, axis=2)[..., None]
    new_keys = jnp.where(hit_rows, written[..., :head_width], key_cache)
    new_values = jnp.where(hit_rows, written[..., head_width:], value_cache)
    return (layer_out, new_keys, new_values, log_own)


def solution(mesh):
    placed = (
        P("dp", None, "kv"),
        P("kv"),
        P("kv", "tp"),
        P("kv", "tp"),
        P("kv", "tp"),
        P(),
        P(),
        P(),
        P(),
        P(),
        P("tp", "kv"),
        P("dp", "kv", "tp"),
        P("dp", "kv", "tp"),
        P("dp", "tp", "kv"),
        P("dp"),
        P("dp"),
        P("dp", None),
    )
    return jax.shard_map(
        shards,
        mesh=mesh,
        in_specs=placed,
        out_specs=(
            P("dp", None, "kv"),
            P("dp", "kv", "tp"),
            P("dp", "kv", "tp"),
            P("dp", None, "tp"),
        ),
        check_vma=False,
    )
```

profile of v0, /device:TPU:1, one launch (start us, length us, event | category | flops | bytes accessed | tf_op | source)
XLA Modules:
  0.0 130.6 jit_solution(2430243420172668842)
XLA Ops:
  0.7 0.8 multiply_reduce_fusion.2
  1.6 0.7 fusion.48
  2.3 0.9 fusion.53
  3.3 1.1 fusion.23
  4.5 1.3 %all_to_all.43 = f32[32,1,3106]{2,1,0:T(1,128)} reshape(f32[99392]{0:T(1024)S(1)} %pad_maximum_fusion) | data formatting | bytes 795136 | tf_op jit(solution)/shard_map/all_to_all | solution.py:42
  5.8 11.9 %all-to-all-start = ((f32[32,1,3106]{2,1,0:T(1,128)}), f32[32,1,3106]{2,1,0:T(1,128)S(1)}, u32[]{:S(2)}, u32[]{:S(2)}) async-start(f32[32,1,3106]{2,1,0:T(1,128)} %all_to_all.43), calls=%async_computation | async-start | bytes 819200 | tf_op jit(solution)/shard_map/all_to_all | solution.py:42
  17.7 4.2 %while.11 = (s32[]{:T(128)}, f32[4,16,16]{2,1,0:T(8,128)S(1)}, s32[4,16]{1,0:T(4,128)S(1)}, f32[16,16]{1,0:T(8,128)S(1)}, s32[]{:T(128)}) while((s32[]{:T(128)}, f32[4,16,16]{2,1,0:T(8,128)S(1)}, s32[4,16]{1,0:T(4,128)S(1)}, f32[16,16]{1,0:T(8,128)S(1)}, s32[]{:T(128)}) %tuple.48), condition=%wide.region_6.7_spmd.clone, body=%wide.region_5.6_spmd.clone.sunk | while | flops 199682 | bytes 17725 | solution.py:80
  17.7 0.2 convolution_add_fusion.2
  18.0 0.2 convolution_add_fusion.2
  18.3 0.2 convolution_add_fusion.2
  18.5 0.2 convolution_add_fusion.2
  18.8 0.2 convolution_add_fusion.2
  19.1 0.2 convolution_add_fusion.2
  19.3 0.2 convolution_add_fusion.2
  19.6 0.2 convolution_add_fusion.2
  19.8 0.2 convolution_add_fusion.2
  20.1 0.2 convolution_add_fusion.2
  20.4 0.2 convolution_add_fusion.2
  20.6 0.2 convolution_add_fusion.2
  20.9 0.2 convolution_add_fusion.2
  21.2 0.2 convolution_add_fusion.2
  21.4 0.2 convolution_add_fusion.2
  21.7 0.2 convolution_add_fusion.2
  22.1 0.6 mul.237
  22.9 2.4 %copy.142 = bf16[4,512,512]{1,2,0:T(8,128)(2,1)} copy(bf16[4,512,512]{2,1,0:T(8,128)(2,1)S(1)} %copy-done.2) | data formatting | bytes 4194304 | tf_op args[11]
  25.3 2.8 %copy.144 = bf16[4,512,512]{1,2,0:T(8,128)(2,1)S(1)} copy(bf16[4,512,512]{2,1,0:T(8,128)(2,1)} %param.31) | data formatting | bytes 4194304 | tf_op args[12]
  28.1 3.5 %all-to-all-done = f32[32,1,3106]{2,1,0:T(1,128)S(1)} async-done(((f32[32,1,3106]{2,1,0:T(1,128)}), f32[32,1,3106]{2,1,0:T(1,128)S(1)}, u32[]{:S(2)}, u32[]{:S(2)}) %all-to-all-start) | async-done | bytes 397600 | tf_op jit(solution)/shard_map/all_to_all | solution.py:42
  31.6 0.2 reduce_sum.108
  31.9 1.0 broadcast_in_dim.148
  32.8 5.7 %all-to-all-start.1 = ((f32[32,1,3106]{2,1,0:T(1,128)}), f32[32,1,3106]{2,1,0:T(1,128)S(1)}, u32[]{:S(2)}, u32[]{:S(2)}) async-start(f32[32,1,3106]{2,1,0:T(1,128)} %broadcast_in_dim.148), calls=%async_computation.1 | async-start | bytes 819200 | tf_op jit(solution)/shard_map/all_to_all | solution.py:19
  38.7 0.6 fusion.35
  39.3 1.3 fusion.64
  40.6 0.7 select_reduce_fusion
  41.3 10.9 %all-to-all-done.1 = f32[32,1,3106]{2,1,0:T(1,128)S(1)} async-done(((f32[32,1,3106]{2,1,0:T(1,128)}), f32[32,1,3106]{2,1,0:T(1,128)S(1)}, u32[]{:S(2)}, u32[]{:S(2)}) %all-to-all-start.1) | async-done | bytes 397600 | tf_op jit(solution)/shard_map/all_to_all | solution.py:19
  52.1 1.0 reduce.4
  53.4 3.5 %slice.41 = f32[6212,16]{1,0:T(8,128)} reshape(f32[32,3106]{1,0:T(8,128)S(1)} %reduce.4) | data formatting | bytes 795136 | tf_op jit(solution)/shard_map/slice | solution.py:57
  58.7 0.8 reshape.283
  59.4 0.8 fusion.65
  60.6 2.1 %fusion.67 = (f32[4,8,16]{2,1,0:T(8,128)S(1)}, f32[4,8,16,512]{3,2,1,0:T(8,128)S(1)}) fusion(f32[4,8,512]{2,1,0:T(8,128)S(1)} %copy-done.7, bf16[4,512,8,64]{1,3,2,0:T(8,128)(2,1)} %bitcast.63, bf16[4,16,8,64]{3,2,1,0:T(8,128)(2,1)S(1)} %reshape.280, pred[4,512]{1,0:T(4,128)(4,1)S(1)} %copy-done.14), kind=kOutput, calls=%fused_computation.107 | convolution fusion | flops 34602496 | bytes 3280896 | tf_op jit(solution)/shard_map/sphd,skhd->shpk/dot_general | solution.py:204
  62.8 0.3 fusion.15
  63.1 0.2 fusion.68
  63.4 0.7 copy-done.4
  64.2 0.7 fusion.49
  64.9 0.7 copy.166
  65.6 5.6 %all-to-all-start.4 = ((f32[1,64,8]{2,0,1:T(1,128)}), f32[1,64,8]{2,0,1:T(1,128)}, u32[]{:S(2)}, u32[]{:S(2)}) async-start(f32[1,64,8]{2,0,1:T(1,128)} %bitcast.13), calls=%async_computation.4 | async-start | bytes 65536 | tf_op jit(solution)/shard_map/all_to_all | solution.py:230
  71.2 1.4 %fusion.13 = f32[4,16,8,64]{3,1,2,0:T(8,128)S(1)} fusion(bf16[4,512,8,64]{1,3,2,0:T(8,128)(2,1)S(1)} %bitcast.62, f32[4,8,16,512]{3,2,1,0:T(8,128)S(1)} %get-tuple-element.96, f32[4,8,16]{2,1,0:T(8,128)S(1)} %get-tuple-element.95, pred[4,512]{1,0:T(4,128)(4,1)} %get-tuple-element.94, f32[4,16,8]{1,2,0:T(8,128)} %get-tuple-element.80), kind=kOutput, calls=%fused_computation.20 | convolution fusion | flops 34373632 | bytes 3282944 | tf_op jit(solution)/shard_map/shpk,skhd->sphd/dot_general | solution.py:106
  72.6 0.9 slice.73
  73.7 1.4 %copy.165 = f32[4,16,8]{2,1,0:T(8,128)} copy(f32[4,16,8]{1,2,0:T(8,128)} %get-tuple-element.81) | data formatting | bytes 4096 | tf_op jit(solution)/shard_map/broadcast_in_dim;reshape | solution.py:229
  75.1 4.7 %all-to-all-done.4 = f32[1,64,8]{2,0,1:T(1,128)} async-done(((f32[1,64,8]{2,0,1:T(1,128)}), f32[1,64,8]{2,0,1:T(1,128)}, u32[]{:S(2)}, u32[]{:S(2)}) %all-to-all-start.4) | async-done | bytes 2080 | tf_op jit(solution)/shard_map/all_to_all | solution.py:230
  79.8 4.4 %all-to-all-start.3 = ((f32[1,64,8]{2,0,1:T(1,128)}), f32[1,64,8]{2,0,1:T(1,128)S(1)}, u32[]{:S(2)}, u32[]{:S(2)}) async-start(f32[1,64,8]{2,0,1:T(1,128)} %bitcast.9), calls=%async_computation.3 | async-start | bytes 65536 | tf_op jit(solution)/shard_map/all_to_all | solution.py:229
  84.2 1.2 fusion.10
  85.6 0.8 broadcast_in_dim_reshape_reshape.4
  86.4 6.5 %all-to-all-done.3 = f32[1,64,8]{2,0,1:T(1,128)S(1)} async-done(((f32[1,64,8]{2,0,1:T(1,128)}), f32[1,64,8]{2,0,1:T(1,128)S(1)}, u32[]{:S(2)}, u32[]{:S(2)}) %all-to-all-start.3) | async-done | bytes 2080 | tf_op jit(solution)/shard_map/all_to_all | solution.py:229
  92.9 4.0 %all-to-all-start.2 = ((f32[1,64,512]{2,0,1:T(1,128)}), f32[1,64,512]{2,0,1:T(1,128)S(1)}, u32[]{:S(2)}, u32[]{:S(2)}) async-start(f32[1,64,512]{2,0,1:T(1,128)} %broadcast_in_dim_reshape_reshape.4), calls=%async_computation.2 | async-start | bytes 262144 | tf_op jit(solution)/shard_map/all_to_all | solution.py:231
  97.0 3.2 %convolution_convert_fusion = bf16[4,512,1024]{2,1,0:T(8,128)(2,1)} fusion(bf16[4,16,512]{2,1,0:T(8,128)(2,1)S(1)} %bitcast.65, bf16[4,16,512]{2,1,0:T(8,128)(2,1)S(1)} %bitcast.64, s32[4,512]{1,0:T(4,128)S(1)} %copy-done.12), kind=kOutput, calls=%fused_computation.6 | convolution fusion | flops 69500928 | bytes 4333568 | tf_op jit(solution)/shard_map/skp,spc->skc/dot_general | solution.py:259
  100.3 0.8 multiply_reduce_fusion.1
  101.6 4.6 %all-to-all-done.2 = f32[1,64,512]{2,0,1:T(1,128)S(1)} async-done(((f32[1,64,512]{2,0,1:T(1,128)}), f32[1,64,512]{2,0,1:T(1,128)S(1)}, u32[]{:S(2)}, u32[]{:S(2)}) %all-to-all-start.2) | async-done | bytes 131104 | tf_op jit(solution)/shard_map/all_to_all | solution.py:231
  106.8 0.7 broadcast_in_dim.162
  107.5 4.4 %all-to-all-start.5 = ((bf16[32,2,512]{2,1,0:T(2,128)(2,1)}), bf16[32,2,512]{2,1,0:T(2,128)(2,1)S(1)}, u32[]{:S(2)}, u32[]{:S(2)}) async-start(bf16[32,2,512]{2,1,0:T(2,128)(2,1)} %broadcast_in_dim.162), calls=%async_computation.5 | async-start | bytes 131072 | tf_op jit(solution)/shard_map/all_to_all | solution.py:19
  111.9 4.4 %slice_select_fusion = (bf16[4,512,512]{2,1,0:T(8,128)(2,1)}, bf16[4,512,512]{2,1,0:T(8,128)(2,1)}) fusion(bf16[4,512,512]{2,1,0:T(8,128)(2,1)S(1)} %copy-done.1, bf16[4,512,1024]{2,1,0:T(8,128)(2,1)} %convolution_convert_fusion, pred[4,512]{1,0:T(4,128)(4,1)S(1)} %copy-done.16, bf16[4,512,512]{2,1,0:T(8,128)(2,1)} %param.30), kind=kLoop, calls=%fused_computation.7 | loop fusion | flops 2097152 | bytes 12584960 | tf_op jit(solution)/shard_map/jit(_where)/select_n | solution.py:264
  116.4 0.7 copy.151
  117.1 3.7 %all-to-all-done.5 = bf16[32,2,512]{2,1,0:T(2,128)(2,1)S(1)} async-done(((bf16[32,2,512]{2,1,0:T(2,128)(2,1)}), bf16[32,2,512]{2,1,0:T(2,128)(2,1)S(1)}, u32[]{:S(2)}, u32[]{:S(2)}) %all-to-all-start.5) | async-done | bytes 65568 | tf_op jit(solution)/shard_map/all_to_all | solution.py:19
  121.0 8.8 %all_to_all.61 = bf16[2,2,2048]{2,1,0:T(2,128)(2,1)S(1)} all-to-all(bf16[2,2,2048]{2,1,0:T(2,128)(2,1)S(1)} %reshape.291), channel_id=1, replica_groups=mesh['dp'=4,'kv'=32,'tp'=2] {'tp'}, dimensions={0} | all-to-all | bytes 32768 | tf_op jit(solution)/shard_map/all_to_all | solution.py:19
  130.0 0.6 reduce_sum.118
  (125 shorter events, 4.7 us)
Async XLA Ops:
  0.6 120.1 %copy-start = (bf16[512,64]{0,1:T(8,128)(2,1)S(1)}, bf16[512,64]{0,1:T(8,128)(2,1)}, u32[]{:S(2)}) copy-start(bf16[512,64]{0,1:T(8,128)(2,1)} %param.29) | copy-start | bytes 196612
  0.6 17.1 %copy-start.13 = (s32[4,16]{1,0:T(4,128)S(1)}, s32[4,16]{1,0:T(4,128)}, u32[]{:S(2)}) copy-start(s32[4,16]{1,0:T(4,128)} %param.35) | copy-start | bytes 772
  4.4 17.6 %copy-start.20 = (f32[64]{0:T(128)S(1)}, f32[64]{0:T(128)}, u32[]{:S(2)}) copy-start(f32[64]{0:T(128)} %param.26) | copy-start | bytes 772
  4.4 17.7 %copy-start.21 = (f32[64]{0:T(128)S(1)}, f32[64]{0:T(128)}, u32[]{:S(2)}) copy-start(f32[64]{0:T(128)} %param.27) | copy-start | bytes 772
  4.4 17.7 %copy-start.22 = (f32[64]{0:T(128)S(1)}, f32[64]{0:T(128)}, u32[]{:S(2)}) copy-start(f32[64]{0:T(128)} %param.28) | copy-start | bytes 772
  4.4 18.5 %copy-start.2 = (bf16[4,512,512]{2,1,0:T(8,128)(2,1)S(1)}, bf16[4,512,512]{2,1,0:T(8,128)(2,1)}, u32[]{:S(2)}) copy-start(bf16[4,512,512]{2,1,0:T(8,128)(2,1)} %param.30) | copy-start | bytes 6291460
  5.8 25.8 %all-to-all-start = ((f32[32,1,3106]{2,1,0:T(1,128)}), f32[32,1,3106]{2,1,0:T(1,128)S(1)}, u32[]{:S(2)}, u32[]{:S(2)}) async-start(f32[32,1,3106]{2,1,0:T(1,128)} %all_to_all.43), calls=%async_computation | async-start | bytes 819200 | tf_op jit(solution)/shard_map/all_to_all | solution.py:42
  22.9 40.5 %copy-start.10 = (pred[4,16,16]{1,2,0:T(8,128)(4,1)}, pred[4,16,16]{1,2,0:T(8,128)(4,1)S(1)}, u32[]{:S(2)}) copy-start(pred[4,16,16]{1,2,0:T(8,128)(4,1)S(1)} %copy.145) | copy-start | bytes 3076
  25.3 2.8 %copy-start.23 = (s32[4]{0:T(128)S(1)}, s32[4]{0:T(128)}, u32[]{:S(2)}) copy-start(s32[4]{0:T(128)} %param.33) | copy-start | bytes 52
  25.3 2.8 %copy-start.24 = (s32[4]{0:T(128)S(1)}, s32[4]{0:T(128)}, u32[]{:S(2)}) copy-start(s32[4]{0:T(128)} %param.34) | copy-start | bytes 52
  25.3 15.3 %copy-start.7 = (f32[4,8,512]{2,1,0:T(8,128)S(1)}, f32[4,8,512]{2,1,0:T(8,128)}, u32[]{:S(2)}) copy-start(f32[4,8,512]{2,1,0:T(8,128)} %param.32) | copy-start | bytes 196612
  32.8 19.3 %all-to-all-start.1 = ((f32[32,1,3106]{2,1,0:T(1,128)}), f32[32,1,3106]{2,1,0:T(1,128)S(1)}, u32[]{:S(2)}, u32[]{:S(2)}) async-start(f32[32,1,3106]{2,1,0:T(1,128)} %broadcast_in_dim.148), calls=%async_computation.1 | async-start | bytes 819200 | tf_op jit(solution)/shard_map/all_to_all | solution.py:19
  38.7 14.7 %copy-start.11 = (s32[4,512]{1,0:T(4,128)}, s32[4,512]{1,0:T(4,128)S(1)}, u32[]{:S(2)}) copy-start(s32[4,512]{1,0:T(4,128)S(1)} %broadcast_subtract_fusion) | copy-start | bytes 24580
  57.1 1.6 %copy-start.3 = (f32[64,1536]{1,0:T(8,128)}, f32[64,1536]{1,0:T(8,128)S(1)}, u32[]{:S(2)}) copy-start(f32[64,1536]{1,0:T(8,128)S(1)} %broadcast_multiply_fusion) | copy-start | bytes 1179652
  57.1 2.3 %copy-start.19 = (f32[16]{0:T(128)S(1)}, f32[16]{0:T(128)}, u32[]{:S(2)}) copy-start(f32[16]{0:T(128)} %param.25) | copy-start | bytes 196
  57.1 3.5 %copy-start.14 = (pred[4,512]{1,0:T(4,128)(4,1)S(1)}, pred[4,512]{1,0:T(4,128)(4,1)}, u32[]{:S(2)}) copy-start(pred[4,512]{1,0:T(4,128)(4,1)} %get-tuple-element.94) | copy-start | bytes 6148
  60.4 2.7 %copy-start.5 = (f32[64,8]{1,0:T(8,128)}, f32[64,8]{1,0:T(8,128)S(1)}, u32[]{:S(2)}) copy-start(f32[64,8]{1,0:T(8,128)S(1)} %fusion.42) | copy-start | bytes 6148
  60.6 2.5 %copy-start.9 = (bf16[4,16,8,64]{3,2,1,0:T(8,128)(2,1)S(1)}, bf16[4,16,8,64]{3,2,1,0:T(8,128)(2,1)}, u32[]{:S(2)}) copy-start(bf16[4,16,8,64]{3,2,1,0:T(8,128)(2,1)} %reshape.283) | copy-start | bytes 196612
  60.6 2.5 %copy-start.18 = (f32[4,8]{1,0:T(4,128)S(1)}, f32[4,8]{1,0:T(4,128)}, u32[]{:S(2)}) copy-start(f32[4,8]{1,0:T(4,128)} %select_reduce_fusion) | copy-start | bytes 388
  60.6 3.5 %copy-start.17 = (pred[4]{0:T(512)(128)(4,1)S(1)}, pred[4]{0:T(512)(128)(4,1)}, u32[]{:S(2)}) copy-start(pred[4]{0:T(512)(128)(4,1)} %get-tuple-element.82) | copy-start | bytes 16
  63.4 0.7 copy-start.4
  63.4 7.8 %copy-start.8 = (f32[4,8,16]{2,1,0:T(8,128)}, f32[4,8,16]{2,1,0:T(8,128)S(1)}, u32[]{:S(2)}) copy-start(f32[4,8,16]{2,1,0:T(8,128)S(1)} %get-tuple-element.97) | copy-start | bytes 6148
  65.6 14.3 %all-to-all-start.4 = ((f32[1,64,8]{2,0,1:T(1,128)}), f32[1,64,8]{2,0,1:T(1,128)}, u32[]{:S(2)}, u32[]{:S(2)}) async-start(f32[1,64,8]{2,0,1:T(1,128)} %bitcast.13), calls=%async_computation.4 | async-start | bytes 65536 | tf_op jit(solution)/shard_map/all_to_all | solution.py:230
  72.6 24.4 %copy-start.12 = (s32[4,512]{1,0:T(4,128)S(1)}, s32[4,512]{1,0:T(4,128)}, u32[]{:S(2)}) copy-start(s32[4,512]{1,0:T(4,128)} %copy-done.11) | copy-start | bytes 24580
  79.8 13.1 %all-to-all-start.3 = ((f32[1,64,8]{2,0,1:T(1,128)}), f32[1,64,8]{2,0,1:T(1,128)S(1)}, u32[]{:S(2)}, u32[]{:S(2)}) async-start(f32[1,64,8]{2,0,1:T(1,128)} %bitcast.9), calls=%async_computation.3 | async-start | bytes 65536 | tf_op jit(solution)/shard_map/all_to_all | solution.py:229
  92.9 13.3 %all-to-all-start.2 = ((f32[1,64,512]{2,0,1:T(1,128)}), f32[1,64,512]{2,0,1:T(1,128)S(1)}, u32[]{:S(2)}, u32[]{:S(2)}) async-start(f32[1,64,512]{2,0,1:T(1,128)} %broadcast_in_dim_reshape_reshape.4), calls=%async_computation.2 | async-start | bytes 262144 | tf_op jit(solution)/shard_map/all_to_all | solution.py:231
  97.0 9.8 %copy-start.15 = (f32[512]{0:T(512)S(1)}, f32[512]{0:T(512)}, u32[]{:S(2)}) copy-start(f32[512]{0:T(512)} %mul.237) | copy-start | bytes 6148
  97.0 14.9 %copy-start.1 = (bf16[4,512,512]{2,1,0:T(8,128)(2,1)S(1)}, bf16[4,512,512]{2,1,0:T(8,128)(2,1)}, u32[]{:S(2)}) copy-start(bf16[4,512,512]{2,1,0:T(8,128)(2,1)} %param.31) | copy-start | bytes 6291460
  97.0 14.9 %copy-start.16 = (pred[4,512]{1,0:T(4,128)(4,1)S(1)}, pred[4,512]{1,0:T(4,128)(4,1)}, u32[]{:S(2)}) copy-start(pred[4,512]{1,0:T(4,128)(4,1)} %fusion.35) | copy-start | bytes 6148
  107.5 13.2 %all-to-all-start.5 = ((bf16[32,2,512]{2,1,0:T(2,128)(2,1)}), bf16[32,2,512]{2,1,0:T(2,128)(2,1)S(1)}, u32[]{:S(2)}, u32[]{:S(2)}) async-start(bf16[32,2,512]{2,1,0:T(2,128)(2,1)} %broadcast_in_dim.162), calls=%async_computation.5 | async-start | bytes 131072 | tf_op jit(solution)/shard_map/all_to_all | solution.py:19
  111.9 4.5 %copy-start.6 = (f32[64,8]{1,0:T(8,128)S(1)}, f32[64,8]{1,0:T(8,128)}, u32[]{:S(2)}) copy-start(f32[64,8]{1,0:T(8,128)} %copy-done.5) | copy-start | bytes 6148
where the time goes:
time: 132 us; the launch traced here: 131 us
  starting transfers between devices  36 us (27%)
  waiting for transfers between devices  34 us (26%)
  local copies, waits for them, and re-layouts  21.5 us (16%)
  other arithmetic  14.3 us (11%)
  matrix products  14.2 us (11%)
  blocking collectives  8.85 us (7%)
    all_to_all x2, waiting for transfers between devices, from_everyone(): lax.all_to_all(jnp.broadcast_to(array[None], (devices, *array.shape)), ax...  14.6 us
    all_to_all x1, starting transfers between devices, summed_on_arrival(): lax.all_to_all(parts, axis, split_axis=0, concat_axis=0, tiled=True)  11.9 us
    all_to_all x2, starting transfers between devices, from_everyone(): lax.all_to_all(jnp.broadcast_to(array[None], (devices, *array.shape)), ax...  10.1 us
    all_to_all x1, blocking collectives, from_everyone(): lax.all_to_all(jnp.broadcast_to(array[None], (devices, *array.shape)), ax...  8.85 us
    all_to_all x1, waiting for transfers between devices, shards(): lax.all_to_all(flat_max[None], 'kv', split_axis=1, concat_axis=0, tiled=T...  6.53 us
    unnamed x54, local copies, waits for them, and re-layouts  6.18 us
    all_to_all x1, starting transfers between devices, shards(): lax.all_to_all(flat_total[None], 'kv', split_axis=1, concat_axis=0, tiled...  5.57 us
    all_to_all x1, waiting for transfers between devices, shards(): lax.all_to_all(flat_total[None], 'kv', split_axis=1, concat_axis=0, tiled...  4.74 us
  transfers between devices with their start and end apart: 6, of which 6 were waited for; matrix products, arithmetic and copies ran while one was open for 22% of the time, Pallas kernels for 0%

commit v1 on v0

v1 whole, which is shorter than its diff:
```python
import jax
import jax.numpy as jnp
from jax import lax
from jax.experimental import pallas as pl
from jax.experimental.pallas import tpu as pltpu
from jax.sharding import PartitionSpec as P

EPSILON = 1e-06
MASKED = -1e30
F32 = jnp.float32
BF16 = jnp.bfloat16

LANES = 128
SUB = 8
N_KV = 32
GROUPS = 8
QUARTERS = 4
ROWS = 64
HEADS = 8
DH = 64
WIDTH = 512
PROPS = 16
SEQS = 4
BLOCK = 512
SEND_A = 26
SEND_B = 32
SEND_C = 16


def iota(shape, dim):
    return lax.broadcasted_iota(jnp.int32, shape, dim)


def dot_nn(a, b):
    return lax.dot_general(a, b, (((1,), (0,)), ((), ())), preferred_element_type=F32)


def dot_nt(a, b):
    return lax.dot_general(a, b, (((1,), (1,)), ((), ())), preferred_element_type=F32)


def pieces(x):
    high = x.astype(BF16).astype(F32)
    rest = x - high
    middle = rest.astype(BF16).astype(F32)
    return high, middle, rest - middle


def vmem():
    return pl.BlockSpec(memory_space=pltpu.VMEM)


def stay(array):
    return pltpu.with_memory_space_constraint(array, pltpu.HBM)


def close(array):
    return pltpu.with_memory_space_constraint(array, pltpu.VMEM)


def hbm():
    return pl.BlockSpec(memory_space=pltpu.HBM)


def smem():
    return pl.BlockSpec(memory_space=pltpu.SMEM)


def cost(flops, moved):
    return pl.CostEstimate(flops=flops, bytes_accessed=moved, transcendentals=0)


def doubled(gain_ref):
    gain = gain_ref[...]
    return jnp.concatenate([gain, gain], axis=1)


def project_kernel(
    x_hbm, gain_hbm, wq_hbm, wk_hbm, wv_hbm, wf_hbm, qgain_hbm, kgain_hbm, hgain_hbm, bias_hbm,
    out_ref, consts_ref,
    x_ref, gain_ref, wq_ref, wk_ref, wv_ref, wf_ref, qgain_ref, kgain_ref, hgain_ref, bias_ref, sems,
):
    kv = lax.axis_index("kv")
    tp = lax.axis_index("tp")
    column = pl.multiple_of(lax.div(kv, 2) * LANES, LANES)
    pairs = (
        (x_hbm, x_ref),
        (gain_hbm, gain_ref),
        (wq_hbm, wq_ref),
        (wk_hbm, wk_ref),
        (wv_hbm, wv_ref),
        (wf_hbm.at[:, pl.ds(column, LANES)], wf_ref),
        (qgain_hbm, qgain_ref),
        (kgain_hbm, kgain_ref),
        (hgain_hbm, hgain_ref),
        (bias_hbm, bias_ref),
    )
    copies = [pltpu.make_async_copy(a, b, sems.at[n]) for n, (a, b) in enumerate(pairs)]
    for copy in copies:
        copy.start()
    for copy in copies:
        copy.wait()
    at = tp * HEADS + 2 * lax.rem(kv, QUARTERS)
    spot = iota((1, 2 * HEADS), 1)
    left = iota((1, LANES), 1) < DH
    first = jnp.sum(jnp.where(spot == at, bias_ref[...], 0.0), axis=1, keepdims=True)
    second = jnp.sum(jnp.where(spot == at + 1, bias_ref[...], 0.0), axis=1, keepdims=True)
    consts_ref[0:1] = doubled(qgain_ref)
    consts_ref[1:2] = doubled(kgain_ref)
    consts_ref[2:3] = doubled(hgain_ref)
    consts_ref[3:4] = jnp.where(left, first, second)
    x = x_ref[...].reshape(ROWS, DH).astype(F32)
    scaled = (x * gain_ref[...]).astype(BF16)
    blocks = [dot_nn(scaled, w[...]) for w in (wq_ref, wk_ref, wv_ref)]
    wide = jnp.concatenate([scaled, scaled], axis=1)
    half = (iota((ROWS, LANES), 1) // DH == lax.rem(kv, 2)).astype(F32).astype(BF16)
    gates = dot_nt(wf_ref[...], wide * half)
    own = jnp.where(tp == 0, gates[:HEADS], gates[HEADS:])
    squares = jnp.sum(x * x, axis=1, keepdims=True)
    diagonal = iota((ROWS, LANES), 0) == iota((ROWS, LANES), 1)
    square_row = jnp.sum(jnp.where(diagonal, squares, 0.0), axis=0, keepdims=True)
    for c in range(QUARTERS):
        gate_row = jnp.concatenate([own[2 * c : 2 * c + 1], own[2 * c + 1 : 2 * c + 2]], axis=1)
        tail = jnp.concatenate([gate_row, square_row], axis=0)
        for g in range(GROUPS):
            at = SEND_A * (g * QUARTERS + c)
            for i, block in enumerate(blocks):
                out_ref[at + SUB * i : at + SUB * i + SUB, :] = block[
                    SUB * g : SUB * g + SUB, LANES * c : LANES * c + LANES
                ]
            out_ref[at + 24 : at + 26, :] = tail


def head_scale(block):
    left = iota(block.shape, 1) < DH
    square = block * block
    first = jnp.sum(jnp.where(left, square, 0.0), axis=1, keepdims=True)
    second = jnp.sum(jnp.where(left, 0.0, square), axis=1, keepdims=True)
    return lax.rsqrt(jnp.where(left, first, second) / DH + EPSILON)


def finish_kernel(got_ref, consts_ref, out_ref, gate_ref):
    group = lax.div(lax.axis_index("kv"), QUARTERS)
    sums = [got_ref[0:8], got_ref[8:16], got_ref[16:24], got_ref[24:26]]
    for p in range(1, N_KV):
        at = SEND_A * p
        for i in range(3):
            sums[i] = sums[i] + got_ref[at + SUB * i : at + SUB * i + SUB]
        sums[3] = sums[3] + got_ref[at + 24 : at + 26]
    gate_sum = sums[3][0:1]
    square = sums[3][1:2]
    inverse_row = lax.rsqrt(square / (N_KV * DH) + EPSILON)
    lane = iota((SUB, LANES), 1)
    pick = lane == iota((SUB, LANES), 0) + group * SUB
    inverse = jnp.sum(jnp.where(pick, inverse_row, 0.0), axis=1, keepdims=True)
    query = sums[0] * inverse
    key = sums[1] * inverse
    value = sums[2] * inverse
    query = query * head_scale(query) * consts_ref[0:1]
    key = key * head_scale(key) * consts_ref[1:2]
    twice = jnp.concatenate([inverse_row[:, :DH], inverse_row[:, :DH]], axis=1)
    logit = gate_sum * twice + consts_ref[3:4]
    small = jnp.exp(-jnp.abs(logit))
    one_more = 1.0 + small
    grown = jnp.where(
        one_more == 1.0, small, jnp.log(one_more) * small / jnp.where(one_more == 1.0, 1.0, one_more - 1.0)
    )
    gate = jnp.minimum(logit, 0.0) - grown
    gate_ref[...] = gate
    high, middle, low = pieces(gate)
    row = iota((SUB, LANES), 0)
    tail = jnp.where(row == 0, high, jnp.where(row == 1, middle, jnp.where(row == 2, low, 0.0)))
    whole = jnp.concatenate([query, key, value, tail], axis=0).astype(BF16)
    for p in range(N_KV):
        out_ref[p] = whole


def stage_kernel(key_hbm, value_hbm, gate_hbm, key_ref, value_ref, gate_ref, new_key_hbm, new_value_hbm, sems):
    loads = []
    for s in range(SEQS):
        for n, (source, target) in enumerate(((key_hbm, key_ref), (value_hbm, value_ref))):
            loads.append(pltpu.make_async_copy(source.at[s], target.at[s], sems.at[n, s]))
    gate_load = pltpu.make_async_copy(gate_hbm, gate_ref, sems.at[4, 0])
    for load in loads:
        load.start()
    gate_load.start()
    stores = []
    for s in range(SEQS):
        for n, (source, target) in enumerate(((key_ref, new_key_hbm), (value_ref, new_value_hbm))):
            loads[2 * s + n].wait()
            store = pltpu.make_async_copy(source.at[s], target.at[s], sems.at[2 + n, s])
            store.start()
            stores.append(store)
    gate_load.wait()
    for store in stores:
        store.wait()


def attend_kernel(lengths_ref, accepted_ref, got_ref, key_ref, value_ref, gate_ref, out_ref):
    for s in range(SEQS):
        attend_sequence(
            s, lengths_ref[s] + accepted_ref[s], got_ref, key_ref, value_ref, gate_ref, out_ref
        )


def attend_sequence(s, base, got_ref, key_ref, value_ref, gate_ref, out_ref):
    kv = lax.axis_index("kv")
    peer = s * 2 * QUARTERS
    query = jnp.concatenate(
        [
            jnp.concatenate([got_ref[peer + c, 0:SUB], got_ref[peer + QUARTERS + c, 0:SUB]], axis=0)
            for c in range(QUARTERS)
        ],
        axis=1,
    )
    wide = (HEADS * PROPS, WIDTH)
    own_head = iota(wide, 0) // PROPS == iota(wide, 1) // DH
    mask = jnp.where(own_head, 0.125, 0.0).astype(BF16)
    spread = jnp.concatenate([query] * HEADS, axis=0) * mask
    scores = dot_nt(spread, key_ref[s])
    gate = gate_ref[s]
    edge_hit = iota((HEADS, BLOCK), 1) + kv * BLOCK == base - 1
    edge = jnp.sum(jnp.where(edge_hit, gate, 0.0), axis=1, keepdims=True)
    gates = jnp.concatenate(
        [jnp.broadcast_to(gate[h : h + 1], (PROPS, BLOCK)) for h in range(HEADS)], axis=0
    )
    position = iota((HEADS * PROPS, BLOCK), 1) + kv * BLOCK
    live = position < base
    scores = jnp.where(live, scores - gates, MASKED)
    peak = jnp.max(scores, axis=1, keepdims=True)
    weights = jnp.where(live, jnp.exp(scores - peak), 0.0)
    total = jnp.sum(weights, axis=1, keepdims=True)
    weighted = dot_nn(weights.astype(BF16), value_ref[s])
    some = total > 0.0
    safe = jnp.where(some, total, 1.0)
    weighted = weighted * (1.0 / safe)
    log_sum = jnp.where(some, peak + jnp.log(safe), MASKED)
    lane = iota((PROPS, WIDTH), 1) // DH
    joined = jnp.zeros((PROPS, WIDTH), F32)
    for h in range(HEADS):
        joined = jnp.where(lane == h, weighted[h * PROPS : (h + 1) * PROPS], joined)
    narrow = iota((PROPS, LANES), 1)
    even = lax.rem(narrow, 2) == 0
    slot = narrow // 2
    for c in range(QUARTERS):
        first = slice(2 * c * PROPS, (2 * c + 1) * PROPS)
        second = slice((2 * c + 1) * PROPS, (2 * c + 2) * PROPS)
        sums = pieces(jnp.where(even, log_sum[first], log_sum[second]))
        edges = pieces(jnp.where(even, edge[2 * c : 2 * c + 1], edge[2 * c + 1 : 2 * c + 2]))
        extra = jnp.zeros((PROPS, LANES), F32)
        for i, piece in enumerate(sums + edges):
            extra = jnp.where(slot == i, piece, extra)
        part = joined[:, LANES * c : LANES * c + LANES]
        for e in range(2):
            out_ref[peer + e * QUARTERS + c] = jnp.concatenate(
                [part[SUB * e : SUB * e + SUB], extra[SUB * e : SUB * e + SUB]], axis=0
            ).astype(BF16)


def tree_kernel(parents_ref, gate_ref, got_ref, out_ref, gates_ref):
    kv = lax.axis_index("kv")
    group = lax.div(kv, QUARTERS)
    quarter = lax.rem(kv, QUARTERS)
    s = lax.div(group, 2)
    half = lax.rem(group, 2)
    square = (PROPS, PROPS)
    parents = parents_ref[pl.ds(s, 1), :]
    step = (iota(square, 0) == parents).astype(F32)
    identity = (iota(square, 0) == iota(square, 1)).astype(F32)
    above = identity + step
    reach = step
    for _ in range(3):
        reach = dot_nn(reach, reach)
        above = above + dot_nn(above, reach)
    lane = iota((2 * PROPS, LANES), 1)
    line = iota((2 * PROPS, LANES), 0)
    wanted = lane == (line // PROPS) * DH + s * PROPS + lax.rem(line, PROPS)
    gate = jnp.sum(jnp.where(wanted, gate_ref[...], 0.0), axis=1, keepdims=True)
    path = [
        jnp.sum(above * gate[PROPS * j : PROPS * j + PROPS], axis=0, keepdims=True) for j in range(2)
    ]
    query = got_ref[group * QUARTERS + quarter, 0:SUB].astype(F32)
    upper = s * 2 * QUARTERS + quarter
    lower = upper + QUARTERS
    keys = jnp.concatenate([got_ref[upper, 8:16], got_ref[lower, 8:16]], axis=0)
    values = jnp.concatenate([got_ref[upper, 16:24], got_ref[lower, 16:24]], axis=0)
    left = iota((SUB, LANES), 1) < DH
    spread = jnp.concatenate([jnp.where(left, query, 0.0), jnp.where(left, 0.0, query)], axis=0)
    scores = dot_nt(spread.astype(BF16), keys) * 0.125
    first = iota(square, 0) < SUB
    scores = scores - jnp.where(first, path[0], path[1])
    chosen = (iota(square, 1) == lax.rem(iota(square, 0), SUB) + half * SUB).astype(F32)
    live = dot_nt(chosen, above) > 0.5
    scores = jnp.where(live, scores, MASKED)
    peak = jnp.max(scores, axis=1, keepdims=True)
    weights = jnp.where(live, jnp.exp(scores - peak), 0.0)
    total = jnp.sum(weights, axis=1, keepdims=True)
    weighted = dot_nn(weights.astype(BF16), values) / total
    log_sum = peak + jnp.log(total)
    out_ref[0:SUB] = jnp.where(left, weighted[:SUB], weighted[SUB:])
    out_ref[SUB:] = jnp.where(left, log_sum[:SUB], log_sum[SUB:])
    for c in range(QUARTERS):
        gate = jnp.sum(got_ref[c, 24:32].astype(F32), axis=0, keepdims=True)
        for j in range(2):
            for t in range(SEQS):
                at = DH * j + PROPS * t
                gates_ref[t, 2 * c + j : 2 * c + j + 1, :] = gate[:, at : at + PROPS]


def merge_kernel(got_ref, tree_ref, consts_ref, out_ref):
    shape = (LANES, LANES)
    source = iota(shape, 0)
    place = iota(shape, 1) // DH
    mine = lax.rem(source, 2) == place
    slot = source // 2
    sums_of = jnp.where(mine & (slot < 3), 1.0, 0.0).astype(BF16)
    edges_of = jnp.where(mine & (slot >= 3) & (slot < 6), 1.0, 0.0).astype(BF16)
    extra = got_ref[:, SUB:, :].reshape(N_KV * SUB, LANES)
    log_sums = dot_nn(extra, sums_of)
    edges = dot_nn(extra, edges_of)
    edge = edges[0:SUB]
    top = log_sums[0:SUB]
    for p in range(1, N_KV):
        edge = edge + edges[SUB * p : SUB * p + SUB]
        top = jnp.maximum(top, log_sums[SUB * p : SUB * p + SUB])
    tree_sum = tree_ref[SUB:] - edge
    top = jnp.maximum(top, tree_sum)
    weight = jnp.exp(tree_sum - top)
    below = weight
    above = weight * tree_ref[0:SUB]
    for p in range(N_KV):
        weight = jnp.exp(log_sums[SUB * p : SUB * p + SUB] - top)
        below = below + weight
        above = above + weight * got_ref[p, 0:SUB].astype(F32)
    attended = above / below
    normed = (attended * head_scale(attended) * consts_ref[2:3]).astype(BF16)
    for p in range(N_KV):
        out_ref[p] = normed


def out_kernel(got_ref, w_ref, out_ref):
    result = jnp.zeros((ROWS, DH), F32)
    for c in range(QUARTERS):
        rows = jnp.concatenate(
            [got_ref[g * QUARTERS + c].astype(F32) for g in range(GROUPS)], axis=0
        ).astype(BF16)
        result = result + dot_nt(rows, w_ref[:, LANES * c : LANES * c + LANES])
    out_ref[...] = result.astype(BF16)


def write_kernel(
    lengths_ref, accepted_ref, got_ref, key_ref, value_ref, _k, _v, new_key_hbm, new_value_hbm, rows_ref, sems
):
    kv = lax.axis_index("kv")
    window = 2 * PROPS
    for s in range(SEQS):
        first = lengths_ref[s] + accepted_ref[s] - kv * BLOCK

        @pl.when((first > -PROPS) & (first < BLOCK))
        def _():
            start = jnp.minimum(lax.div(jnp.maximum(first, 0), PROPS) * PROPS, BLOCK - window)
            start = pl.multiple_of(start, PROPS)
            slot = iota((window, PROPS), 0) + start - first
            placing = (slot == iota((window, PROPS), 1)).astype(F32).astype(BF16)
            line = iota((window, WIDTH), 0) + start - first
            hit = (line >= 0) & (line < PROPS)
            copies = []
            for i, (old_ref, new_hbm) in enumerate(((key_ref, new_key_hbm), (value_ref, new_value_hbm))):
                at = SUB * (i + 1)
                rows = jnp.concatenate(
                    [
                        jnp.concatenate(
                            [
                                got_ref[2 * s * QUARTERS + c, at : at + SUB],
                                got_ref[(2 * s + 1) * QUARTERS + c, at : at + SUB],
                            ],
                            axis=0,
                        )
                        for c in range(QUARTERS)
                    ],
                    axis=1,
                )
                written = dot_nn(placing, rows)
                old = old_ref[s, pl.ds(start, window), :].astype(F32)
                rows_ref[2 * s + i] = jnp.where(hit, written, old).astype(BF16)
                copies.append(
                    pltpu.make_async_copy(
                        rows_ref.at[2 * s + i], new_hbm.at[s, pl.ds(start, window), :], sems.at[i]
                    )
                )
            for copy in copies:
                copy.start()
            for copy in copies:
                copy.wait()


def exchange(array):
    return lax.all_to_all(array, "kv", split_axis=0, concat_axis=0, tiled=True)


def shards(
    tokens,
    norm_gain,
    w_query,
    w_key,
    w_value,
    w_forget,
    forget_bias,
    query_gain,
    key_gain,
    head_gain,
    w_out,
    key_cache,
    value_cache,
    gate_cache,
    lengths,
    accepted,
    parents,
):
    def line(gain):
        return gain.reshape(1, DH)

    def limit(size):
        return pltpu.CompilerParams(vmem_limit_bytes=size * 2**20)

    cache = jax.ShapeDtypeStruct(key_cache.shape, BF16)
    sent, consts = pl.pallas_call(
        project_kernel,
        out_shape=(
            jax.ShapeDtypeStruct((N_KV * SEND_A, LANES), F32),
            jax.ShapeDtypeStruct((SUB, LANES), F32),
        ),
        in_specs=[hbm()] * 10,
        out_specs=(vmem(), vmem()),
        scratch_shapes=[
            pltpu.VMEM((SEQS, PROPS, DH), BF16),
            pltpu.VMEM((1, DH), F32),
            pltpu.VMEM((DH, WIDTH), BF16),
            pltpu.VMEM((DH, WIDTH), BF16),
            pltpu.VMEM((DH, WIDTH), BF16),
            pltpu.VMEM((2 * HEADS, LANES), BF16),
            pltpu.VMEM((1, DH), F32),
            pltpu.VMEM((1, DH), F32),
            pltpu.VMEM((1, DH), F32),
            pltpu.VMEM((1, 2 * HEADS), F32),
            pltpu.SemaphoreType.DMA((10,)),
        ],
        cost_estimate=cost(13_000_000, 700_000),
        compiler_params=limit(8),
        name="project",
    )(
        *map(
            stay,
            (
                tokens, line(norm_gain), w_query, w_key, w_value, w_forget.T,
                line(query_gain), line(key_gain), line(head_gain), forget_bias.reshape(1, 2 * HEADS),
            ),
        )
    )
    got = exchange(sent.reshape(N_KV, 1, SEND_A * LANES)).reshape(N_KV * SEND_A, LANES)
    consts, key_cache, value_cache, gate_cache = lax.optimization_barrier(
        (consts, key_cache, value_cache, gate_cache)
    )
    keys, values, gate_block, new_keys, new_values = pl.pallas_call(
        stage_kernel,
        out_shape=(
            pltpu.VMEM(key_cache.shape, BF16),
            pltpu.VMEM(value_cache.shape, BF16),
            jax.ShapeDtypeStruct(gate_cache.shape, F32),
            pltpu.HBM(key_cache.shape, BF16),
            pltpu.HBM(value_cache.shape, BF16),
        ),
        in_specs=[hbm()] * 3,
        out_specs=(vmem(), vmem(), vmem(), hbm(), hbm()),
        scratch_shapes=[pltpu.SemaphoreType.DMA((5, SEQS))],
        cost_estimate=cost(500_000_000, 8_500_000),
        compiler_params=limit(8),
        name="stage",
    )(stay(key_cache), stay(value_cache), stay(gate_cache))
    got, keys, values = lax.optimization_barrier((got, keys, values))
    sent, gate_row = pl.pallas_call(
        finish_kernel,
        out_shape=(
            jax.ShapeDtypeStruct((N_KV, SEND_B, LANES), BF16),
            jax.ShapeDtypeStruct((1, LANES), F32),
        ),
        in_specs=[vmem(), vmem()],
        out_specs=(vmem(), vmem()),
        cost_estimate=cost(1_000_000, 700_000),
        compiler_params=limit(8),
        name="finish",
    )(got, consts)
    rows = exchange(sent)
    sent = pl.pallas_call(
        attend_kernel,
        out_shape=jax.ShapeDtypeStruct((N_KV, SEND_C, LANES), BF16),
        in_specs=[smem(), smem()] + [vmem()] * 4,
        out_specs=vmem(),
        cost_estimate=cost(600_000_000, 4_500_000),
        compiler_params=limit(16),
        name="attend",
    )(lengths, accepted, rows, close(keys), close(values), gate_block)
    got = exchange(sent)
    tree, gates = pl.pallas_call(
        tree_kernel,
        out_shape=(
            jax.ShapeDtypeStruct((2 * SUB, LANES), F32),
            jax.ShapeDtypeStruct((SEQS, HEADS, PROPS), F32),
        ),
        in_specs=[vmem()] * 3,
        out_specs=(vmem(), vmem()),
        cost_estimate=cost(2_000_000, 300_000),
        compiler_params=limit(8),
        name="tree",
    )(parents, gate_row, rows)
    new_keys, new_values = pl.pallas_call(
        write_kernel,
        out_shape=(cache, cache),
        in_specs=[smem(), smem(), vmem(), vmem(), vmem(), hbm(), hbm()],
        out_specs=(hbm(), hbm()),
        scratch_shapes=[
            pltpu.VMEM((2 * SEQS, 2 * PROPS, WIDTH), BF16),
            pltpu.SemaphoreType.DMA((2,)),
        ],
        input_output_aliases={5: 0, 6: 1},
        cost_estimate=cost(60_000_000, 8_500_000),
        compiler_params=limit(8),
        name="write",
    )(lengths, accepted, rows, close(keys), close(values), stay(new_keys), stay(new_values))
    tree, new_keys, new_values = lax.optimization_barrier((tree, new_keys, new_values))
    sent = pl.pallas_call(
        merge_kernel,
        out_shape=jax.ShapeDtypeStruct((N_KV, SUB, LANES), BF16),
        in_specs=[vmem()] * 3,
        out_specs=vmem(),
        cost_estimate=cost(8_000_000, 200_000),
        compiler_params=limit(8),
        name="merge",
    )(got, tree, consts)
    got = exchange(sent)
    term = pl.pallas_call(
        out_kernel,
        out_shape=jax.ShapeDtypeStruct((ROWS, DH), BF16),
        in_specs=[vmem()] * 2,
        out_specs=vmem(),
        cost_estimate=cost(4_000_000, 150_000),
        compiler_params=limit(8),
        name="out",
    )(got, w_out.T)
    other = lax.ppermute(term, "tp", [(0, 1), (1, 0)])
    layer_out = (term.astype(F32) + other.astype(F32)).astype(BF16)
    return (layer_out.reshape(SEQS, PROPS, DH), new_keys, new_values, gates.transpose(0, 2, 1))


def solution(mesh):
    placed = (
        P("dp", None, "kv"),
        P("kv"),
        P("kv", "tp"),
        P("kv", "tp"),
        P("kv", "tp"),
        P(),
        P(),
        P(),
        P(),
        P(),
        P("tp", "kv"),
        P("dp", "kv", "tp"),
        P("dp", "kv", "tp"),
        P("dp", "tp", "kv"),
        P("dp"),
        P("dp"),
        P("dp", None),
    )
    return jax.shard_map(
        shards,
        mesh=mesh,
        in_specs=placed,
        out_specs=(
            P("dp", None, "kv"),
            P("dp", "kv", "tp"),
            P("dp", "kv", "tp"),
            P("dp", None, "tp"),
        ),
        check_vma=False,
    )
```

time: 132 us -> 82.9 us (0.63)
  blocking collectives: 8.85 us -> 28 us
  waiting for transfers between devices: 34 us -> 15.5 us
  local copies, waits for them, and re-layouts: 21.5 us -> 4.53 us
  matrix products: 14.2 us -> 0 us
  starting transfers between devices: 36 us -> 21.8 us
  other arithmetic: 14.3 us -> 0.61 us
  Pallas kernels: 0 us -> 11.4 us
    all_to_all x6 -> x2, waiting for transfers between devices: 34 us -> 14.6 us  [exchange(): return lax.all_to_all(array, 'kv', split_axis=0, concat_axis=0, tiled=True)]
    all_to_all x1 -> x2, blocking collectives: 8.85 us -> 28 us  [exchange(): return lax.all_to_all(array, 'kv', split_axis=0, concat_axis=0, tiled=True)]
    all_to_all x6 -> x2, starting transfers between devices: 36 us -> 17 us  [exchange(): return lax.all_to_all(array, 'kv', split_axis=0, concat_axis=0, tiled=True)]
    dot_general x25 -> x0, matrix products: 14.2 us -> none  [the longest x16 3.68 us: extend(): jnp.einsum('sij,sjk->sik', step_matrix, ancestors, precision=lax.Precisio...]
    pallas_call x0 -> x8, Pallas kernels: none -> 11.4 us  [the longest x1 3.62 us: shards(): pl.pallas_call(stage_kernel, out_shape=(pltpu.VMEM(key_cache.shape, BF16)...]
    ppermute x0 -> x1, starting transfers between devices: none -> 4.81 us  [shards(): other = lax.ppermute(term, 'tp', [(0, 1), (1, 0)])]
    slice x3 -> x0, local copies, waits for them, and re-layouts: 4.48 us -> none  [the longest x2 3.54 us: packed_total(): total[b:e].reshape(a.shape)]
    select_n x1 -> x0, other arithmetic: 4.45 us -> none  [shards(): new_values = jnp.where(hit_rows, written[..., head_width:], value_cache)]
  transfers between devices with their start and end apart: 6 -> 3, of which waited for: 6 -> 3; matrix products, arithmetic and copies ran while one was open for 22% -> 0% of each run, Pallas kernels for 0% -> 7%
where the time goes in v1:
time: 82.9 us; the launch traced here: 82.5 us
  blocking collectives  28 us (34%)
  starting transfers between devices  21.8 us (26%)
  waiting for transfers between devices  15.5 us (19%)
  Pallas kernels  11.4 us (14%)
  local copies, waits for them, and re-layouts  4.53 us (5%)
    all_to_all x2, blocking collectives, exchange(): return lax.all_to_all(array, 'kv', split_axis=0, concat_axis=0, tiled=True)  28 us
    all_to_all x2, starting transfers between devices, exchange(): return lax.all_to_all(array, 'kv', split_axis=0, concat_axis=0, tiled=True)  17 us
    all_to_all x2, waiting for transfers between devices, exchange(): return lax.all_to_all(array, 'kv', split_axis=0, concat_axis=0, tiled=True)  14.6 us
    ppermute x1, starting transfers between devices, shards(): other = lax.ppermute(term, 'tp', [(0, 1), (1, 0)])  4.81 us
    unnamed x14, local copies, waits for them, and re-layouts  4.53 us
    pallas_call x1, Pallas kernels, shards(): pl.pallas_call(stage_kernel, out_shape=(pltpu.VMEM(key_cache.shape, BF16)...  3.62 us
    pallas_call x1, Pallas kernels, shards(): pl.pallas_call(attend_kernel, out_shape=jax.ShapeDtypeStruct((N_KV, SEND_...  3.08 us
    pallas_call x1, Pallas kernels, shards(): pl.pallas_call(project_kernel, out_shape=(jax.ShapeDtypeStruct((N_KV * SE...  2.08 us
  transfers between devices with their start and end apart: 3, of which 3 were waited for; matrix products, arithmetic and copies ran while one was open for 0% of the time, Pallas kernels for 7%

profile of v1, /device:TPU:1, one launch (start us, length us, event | category | flops | bytes accessed | tf_op | source)
XLA Modules:
  0.0 82.5 jit_solution(3780267297226871198)
XLA Ops:
  0.6 2.1 %project.1 = (f32[832,128]{1,0:T(8,128)}, f32[8,128]{1,0:T(8,128)S(1)}) custom-call(bf16[4,16,64]{2,1,0:T(8,128)(2,1)} %x_hbm.1, f32[1,64]{1,0:T(1,128)} %bitcast.15, bf16[64,512]{1,0:T(8,128)(2,1)} %wq_hbm.1, bf16[64,512]{1,0:T(8,128)(2,1)} %wk_hbm.1, bf16[64,512]{1,0:T(8,128)(2,1)} %wv_hbm.1, bf16[16,2048]{1,0:T(8,128)(2,1)} %bitcast.13, ...), custom_call_target="tpu_custom_call" | custom-call | flops 13000000 | bytes 700000 | tf_op jit(solution)/shard_map/project/pallas_call | solution.py:427
  2.7 11.9 %all-to-all-start = ((f32[32,1,3328]{2,1,0:T(1,128)}), f32[32,1,3328]{2,1,0:T(1,128)S(1)}, u32[]{:S(2)}, u32[]{:S(2)}) async-start(f32[32,1,3328]{2,1,0:T(1,128)} %bitcast.6), calls=%async_computation | async-start | bytes 851968 | tf_op jit(solution)/shard_map/all_to_all | solution.py:398
  14.6 0.0 copy-start.5
  14.6 0.0 copy-start.6
  14.6 3.6 %stage.1 = (bf16[4,512,512]{2,1,0:T(8,128)(2,1)S(1)}, bf16[4,512,512]{2,1,0:T(8,128)(2,1)S(1)}, f32[4,8,512]{2,1,0:T(8,128)S(1)}, bf16[4,512,512]{2,1,0:T(8,128)(2,1)}, bf16[4,512,512]{2,1,0:T(8,128)(2,1)}) custom-call(bf16[4,512,512]{2,1,0:T(8,128)(2,1)} %key_hbm, bf16[4,512,512]{2,1,0:T(8,128)(2,1)} %value_hbm, f32[4,8,512]{2,1,0:T(8,128)} %gate_hbm), custom_call_target="tpu_custom_call" | custom-call | flops 500000000 | bytes 8500000 | tf_op jit(solution)/shard_map/stage/pallas_call | solution.py:464
  18.2 0.0 copy-start
  18.3 1.3 %copy-done = bf16[4,512,512]{2,1,0:T(8,128)(2,1)} copy-done((bf16[4,512,512]{2,1,0:T(8,128)(2,1)}, bf16[4,512,512]{2,1,0:T(8,128)(2,1)S(1)}, u32[]{:S(2)}) %copy-start) | copy-done | bytes 2097176
  19.6 8.9 %all-to-all-done = f32[32,1,3328]{2,1,0:T(1,128)S(1)} async-done(((f32[32,1,3328]{2,1,0:T(1,128)}), f32[32,1,3328]{2,1,0:T(1,128)S(1)}, u32[]{:S(2)}, u32[]{:S(2)}) %all-to-all-start) | async-done | bytes 426016 | tf_op jit(solution)/shard_map/all_to_all | solution.py:398
  28.5 0.2 finish.1
  28.7 15.9 %all_to_all.20.got_ref = bf16[32,32,128]{2,1,0:T(8,128)(2,1)S(1)} all-to-all(bf16[32,32,128]{2,1,0:T(8,128)(2,1)S(1)} %get-tuple-element.36), channel_id=1, replica_groups=mesh['dp'=4,'kv'=32,'tp'=2] {'kv'}, dimensions={0} | all-to-all | bytes 524288 | tf_op jit(solution)/shard_map/all_to_all | solution.py:398
  44.5 0.0 copy-done.5
  44.5 0.0 copy-done.6
  44.6 0.0 copy-start.1
  44.6 1.6 %copy-done.1 = bf16[4,512,512]{2,1,0:T(8,128)(2,1)S(1)} copy-done((bf16[4,512,512]{2,1,0:T(8,128)(2,1)S(1)}, bf16[4,512,512]{2,1,0:T(8,128)(2,1)}, u32[]{:S(2)}) %copy-start.1) | copy-done | bytes 2097176
  46.1 0.0 copy-start.4
  46.1 3.1 %attend.1 = bf16[32,16,128]{2,1,0:T(8,128)(2,1)} custom-call(s32[4]{0:T(128)S(1)} %copy-done.5, s32[4]{0:T(128)S(1)} %copy-done.6, bf16[32,32,128]{2,1,0:T(8,128)(2,1)S(1)} %all_to_all.20.got_ref, bf16[4,512,512]{2,1,0:T(8,128)(2,1)S(1)} %get-tuple-element.37.key_ref, bf16[4,512,512]{2,1,0:T(8,128)(2,1)S(1)} %copy-done.1, ...), custom_call_target="tpu_custom_call" | custom-call | flops 600000000 | bytes 4500000 | tf_op jit(solution)/shard_map/attend/pallas_call | solution.py:494
  49.2 5.1 %all-to-all-start.2 = ((bf16[32,16,128]{2,1,0:T(8,128)(2,1)}), bf16[32,16,128]{2,1,0:T(8,128)(2,1)S(1)}, u32[]{:S(2)}, u32[]{:S(2)}) async-start(bf16[32,16,128]{2,1,0:T(8,128)(2,1)} %attend.1), calls=%async_computation.2 | async-start | bytes 262144 | tf_op jit(solution)/shard_map/all_to_all | solution.py:398
  54.3 0.0 copy-done.4
  54.3 1.4 %tree.1 = (f32[16,128]{1,0:T(8,128)S(1)}, f32[4,8,16]{2,1,0:T(8,128)}) custom-call(s32[4,16]{1,0:T(4,128)S(1)} %copy-done.4, f32[1,128]{1,0:T(1,128)S(1)} %get-tuple-element.40.gate_ref, bf16[32,32,128]{2,1,0:T(8,128)(2,1)S(1)} %all_to_all.20.got_ref), custom_call_target="tpu_custom_call" | custom-call | flops 2000000 | bytes 300000 | tf_op jit(solution)/shard_map/tree/pallas_call | solution.py:504
  55.7 0.0 copy-start.2
  55.7 1.6 %copy-done.2 = bf16[4,512,512]{2,1,0:T(8,128)(2,1)S(1)} copy-done((bf16[4,512,512]{2,1,0:T(8,128)(2,1)S(1)}, bf16[4,512,512]{2,1,0:T(8,128)(2,1)}, u32[]{:S(2)}) %copy-start.2) | copy-done | bytes 2097176
  57.3 0.0 copy-start.3
  57.3 0.6 write.1
  57.9 5.8 %all-to-all-done.2.got_ref = bf16[32,16,128]{2,1,0:T(8,128)(2,1)S(1)} async-done(((bf16[32,16,128]{2,1,0:T(8,128)(2,1)}), bf16[32,16,128]{2,1,0:T(8,128)(2,1)S(1)}, u32[]{:S(2)}, u32[]{:S(2)}) %all-to-all-start.2) | async-done | bytes 131104 | tf_op jit(solution)/shard_map/all_to_all | solution.py:398
  63.7 0.3 merge.1
  64.0 12.1 %all_to_all.21.got_ref = bf16[32,8,128]{2,1,0:T(8,128)(2,1)S(1)} all-to-all(bf16[32,8,128]{2,1,0:T(8,128)(2,1)S(1)} %merge.1), channel_id=1, replica_groups=mesh['dp'=4,'kv'=32,'tp'=2] {'kv'}, dimensions={0} | all-to-all | bytes 131072 | tf_op jit(solution)/shard_map/all_to_all | solution.py:398
  76.1 0.0 copy-done.3
  76.1 0.1 out.1
  76.2 4.8 %collective-permute-start = (bf16[64,64]{1,0:T(8,128)(2,1)S(1)}, bf16[64,64]{1,0:T(8,128)(2,1)S(1)}, u32[]{:S(2)}, u32[]{:S(2)}) collective-permute-start(bf16[64,64]{1,0:T(8,128)(2,1)S(1)} %out.1), channel_id=1, source_target_pairs={{0,1},{1,0},{2,3},{3,2},{4,5},{5,4},{6,7},{7,6},{8,9},{9,8},{10,11... | collective-permute-start | bytes 24584 | tf_op jit(solution)/shard_map/ppermute | solution.py:550
  81.1 0.8 %collective-permute-done = bf16[64,64]{1,0:T(8,128)(2,1)S(1)} collective-permute-done((bf16[64,64]{1,0:T(8,128)(2,1)S(1)}, bf16[64,64]{1,0:T(8,128)(2,1)S(1)}, u32[]{:S(2)}, u32[]{:S(2)}) %collective-permute-start) | collective-permute-done | bytes 8224 | tf_op jit(solution)/shard_map/ppermute | solution.py:550
  81.9 0.6 add_convert_fusion
Async XLA Ops:
  2.7 25.7 %all-to-all-start = ((f32[32,1,3328]{2,1,0:T(1,128)}), f32[32,1,3328]{2,1,0:T(1,128)S(1)}, u32[]{:S(2)}, u32[]{:S(2)}) async-start(f32[32,1,3328]{2,1,0:T(1,128)} %bitcast.6), calls=%async_computation | async-start | bytes 851968 | tf_op jit(solution)/shard_map/all_to_all | solution.py:398
  14.6 30.0 %copy-start.5 = (s32[4]{0:T(128)S(1)}, s32[4]{0:T(128)}, u32[]{:S(2)}) copy-start(s32[4]{0:T(128)} %lengths_ref.3) | copy-start | bytes 52
  14.6 29.9 %copy-start.6 = (s32[4]{0:T(128)S(1)}, s32[4]{0:T(128)}, u32[]{:S(2)}) copy-start(s32[4]{0:T(128)} %accepted_ref.3) | copy-start | bytes 52
  18.2 1.3 %copy-start = (bf16[4,512,512]{2,1,0:T(8,128)(2,1)}, bf16[4,512,512]{2,1,0:T(8,128)(2,1)S(1)}, u32[]{:S(2)}) copy-start(bf16[4,512,512]{2,1,0:T(8,128)(2,1)S(1)} %get-tuple-element.38.value_ref) | copy-start | bytes 6291460
  44.6 1.6 %copy-start.1 = (bf16[4,512,512]{2,1,0:T(8,128)(2,1)S(1)}, bf16[4,512,512]{2,1,0:T(8,128)(2,1)}, u32[]{:S(2)}) copy-start(bf16[4,512,512]{2,1,0:T(8,128)(2,1)} %copy-done) | copy-start | bytes 6291460
  46.1 8.2 %copy-start.4 = (s32[4,16]{1,0:T(4,128)S(1)}, s32[4,16]{1,0:T(4,128)}, u32[]{:S(2)}) copy-start(s32[4,16]{1,0:T(4,128)} %parents_ref.1) | copy-start | bytes 772
  49.2 14.5 %all-to-all-start.2 = ((bf16[32,16,128]{2,1,0:T(8,128)(2,1)}), bf16[32,16,128]{2,1,0:T(8,128)(2,1)S(1)}, u32[]{:S(2)}, u32[]{:S(2)}) async-start(bf16[32,16,128]{2,1,0:T(8,128)(2,1)} %attend.1), calls=%async_computation.2 | async-start | bytes 262144 | tf_op jit(solution)/shard_map/all_to_all | solution.py:398
  55.7 1.6 %copy-start.2 = (bf16[4,512,512]{2,1,0:T(8,128)(2,1)S(1)}, bf16[4,512,512]{2,1,0:T(8,128)(2,1)}, u32[]{:S(2)}) copy-start(bf16[4,512,512]{2,1,0:T(8,128)(2,1)} %copy-done) | copy-start | bytes 6291460
  57.3 18.8 %copy-start.3 = (bf16[512,64]{0,1:T(8,128)(2,1)S(1)}, bf16[512,64]{0,1:T(8,128)(2,1)}, u32[]{:S(2)}) copy-start(bf16[512,64]{0,1:T(8,128)(2,1)} %param.27) | copy-start | bytes 196612
  76.2 5.7 %collective-permute-start = (bf16[64,64]{1,0:T(8,128)(2,1)S(1)}, bf16[64,64]{1,0:T(8,128)(2,1)S(1)}, u32[]{:S(2)}, u32[]{:S(2)}) collective-permute-start(bf16[64,64]{1,0:T(8,128)(2,1)S(1)} %out.1), channel_id=1, source_target_pairs={{0,1},{1,0},{2,3},{3,2},{4,5},{5,4},{6,7},{7,6},{8,9},{9,8},{10,11... | collective-permute-start | bytes 24584 | tf_op jit(solution)/shard_map/ppermute | solution.py:550

commit v2 on v1

--- a/solution.py
+++ b/solution.py
@@ -23,8 +23,9 @@
 SEQS = 4
 BLOCK = 512
 SEND_A = 26
-SEND_B = 32
-SEND_C = 16
+SEND_B = 24
+SEND_C = 24
+HELD = 2
 
 
 def iota(shape, dim):
@@ -54,10 +55,6 @@
     return pltpu.with_memory_space_constraint(array, pltpu.HBM)
 
 
-def close(array):
-    return pltpu.with_memory_space_constraint(array, pltpu.VMEM)
-
-
 def hbm():
     return pl.BlockSpec(memory_space=pltpu.HBM)
 
@@ -76,9 +73,9 @@
 
 
 def project_kernel(
-    x_hbm, gain_hbm, wq_hbm, wk_hbm, wv_hbm, wf_hbm, qgain_hbm, kgain_hbm, hgain_hbm, bias_hbm,
+    x_hbm, gain_hbm, wq_hbm, wk_hbm, wv_hbm, wf_hbm, qgain_hbm, kgain_hbm, hgain_hbm, bias_hbm, lengths_hbm, accepted_hbm,
     out_ref, consts_ref,
-    x_ref, gain_ref, wq_ref, wk_ref, wv_ref, wf_ref, qgain_ref, kgain_ref, hgain_ref, bias_ref, sems,
+    x_ref, gain_ref, wq_ref, wk_ref, wv_ref, wf_ref, qgain_ref, kgain_ref, hgain_ref, bias_ref, lengths_ref, accepted_ref, sems,
 ):
     kv = lax.axis_index("kv")
     tp = lax.axis_index("tp")
@@ -94,6 +91,8 @@
         (kgain_hbm, kgain_ref),
         (hgain_hbm, hgain_ref),
         (bias_hbm, bias_ref),
+        (lengths_hbm, lengths_ref),
+        (accepted_hbm, accepted_ref),
     )
     copies = [pltpu.make_async_copy(a, b, sems.at[n]) for n, (a, b) in enumerate(pairs)]
     for copy in copies:
@@ -109,6 +108,7 @@
     consts_ref[1:2] = doubled(kgain_ref)
     consts_ref[2:3] = doubled(hgain_ref)
     consts_ref[3:4] = jnp.where(left, first, second)
+    consts_ref[4:5, 0:SEQS] = (lengths_ref[...] + accepted_ref[...]).astype(F32)
     x = x_ref[...].reshape(ROWS, DH).astype(F32)
     scaled = (x * gain_ref[...]).astype(BF16)
     blocks = [dot_nn(scaled, w[...]) for w in (wq_ref, wk_ref, wv_ref)]
@@ -167,44 +167,66 @@
     )
     gate = jnp.minimum(logit, 0.0) - grown
     gate_ref[...] = gate
-    high, middle, low = pieces(gate)
-    row = iota((SUB, LANES), 0)
-    tail = jnp.where(row == 0, high, jnp.where(row == 1, middle, jnp.where(row == 2, low, 0.0)))
-    whole = jnp.concatenate([query, key, value, tail], axis=0).astype(BF16)
+    whole = jnp.concatenate([query, key, value], axis=0).astype(BF16)
     for p in range(N_KV):
         out_ref[p] = whole
 
 
-def stage_kernel(key_hbm, value_hbm, gate_hbm, key_ref, value_ref, gate_ref, new_key_hbm, new_value_hbm, sems):
-    loads = []
-    for s in range(SEQS):
-        for n, (source, target) in enumerate(((key_hbm, key_ref), (value_hbm, value_ref))):
-            loads.append(pltpu.make_async_copy(source.at[s], target.at[s], sems.at[n, s]))
-    gate_load = pltpu.make_async_copy(gate_hbm, gate_ref, sems.at[4, 0])
+def stage_kernel(
+    key_hbm, value_hbm, gate_hbm, key_ref, held_ref, gate_ref, new_key_hbm, new_value_hbm, rest_ref, sems
+):
+    gate_load = pltpu.make_async_copy(gate_hbm, gate_ref, sems.at[2, 0])
+    gate_load.start()
+    targets = [key_ref.at[s] for s in range(SEQS)]
+    targets += [held_ref.at[s] if s < HELD else rest_ref.at[s - HELD] for s in range(SEQS)]
+    sources = [key_hbm.at[s] for s in range(SEQS)] + [value_hbm.at[s] for s in range(SEQS)]
+    news = [new_key_hbm.at[s] for s in range(SEQS)] + [new_value_hbm.at[s] for s in range(SEQS)]
+    loads = [pltpu.make_async_copy(a, b, sems.at[0, n]) for n, (a, b) in enumerate(zip(sources, targets))]
+    stores = [pltpu.make_async_copy(a, b, sems.at[1, n]) for n, (a, b) in enumerate(zip(targets, news))]
     for load in loads:
         load.start()
-    gate_load.start()
-    stores = []
-    for s in range(SEQS):
-        for n, (source, target) in enumerate(((key_ref, new_key_hbm), (value_ref, new_value_hbm))):
-            loads[2 * s + n].wait()
-            store = pltpu.make_async_copy(source.at[s], target.at[s], sems.at[2 + n, s])
-            store.start()
-            stores.append(store)
+    for load, store in zip(loads, stores):
+        load.wait()
+        store.start()
     gate_load.wait()
     for store in stores:
         store.wait()
 
 
-def attend_kernel(lengths_ref, accepted_ref, got_ref, key_ref, value_ref, gate_ref, out_ref):
+def attend_kernel(
+    consts_ref, row_ref, parents_ref, got_ref, key_ref, held_ref, gate_ref, value_hbm,
+    out_ref, tree_ref, rest_ref, weights_ref, sems,
+):
+    loads = {}
+    for s in range(HELD, SEQS):
+        loads[s] = pltpu.make_async_copy(value_hbm.at[s], rest_ref.at[s - HELD], sems.at[s])
+        loads[s].start()
+    tail = gate_tail(row_ref)
+    attend_tree(parents_ref, row_ref, got_ref, tree_ref)
+    sums = []
     for s in range(SEQS):
-        attend_sequence(
-            s, lengths_ref[s] + accepted_ref[s], got_ref, key_ref, value_ref, gate_ref, out_ref
-        )
-
-
-def attend_sequence(s, base, got_ref, key_ref, value_ref, gate_ref, out_ref):
-    kv = lax.axis_index("kv")
+        raw = score_sequence(s, got_ref, key_ref)
+        sums.append(weigh_sequence(s, raw, consts_ref[4:5, s : s + 1], gate_ref, weights_ref))
+    for s in range(SEQS):
+        if s in loads:
+            loads[s].wait()
+        values = held_ref[s] if s < HELD else rest_ref[s - HELD]
+        send_sequence(s, dot_nn(weights_ref[s], values), *sums[s], tail, out_ref)
+
+
+def gate_tail(row_ref):
+    shape = (LANES, LANES)
+    narrow = lax.rem(iota(shape, 0), PROPS) == lax.rem(iota(shape, 1), PROPS)
+    slot = iota(shape, 1) // PROPS
+    mine = iota((SUB, LANES), 1) // PROPS == iota((SUB, LANES), 0)
+    tail = jnp.zeros((SUB, LANES), F32)
+    for i, piece in enumerate(pieces(row_ref[...])):
+        move = jnp.where(narrow & (slot == i + 1), 1.0, 0.0).astype(BF16)
+        tail = tail + dot_nn(jnp.where(mine, piece, 0.0).astype(BF16), move)
+    return tail
+
+
+def score_sequence(s, got_ref, key_ref):
     peer = s * 2 * QUARTERS
     query = jnp.concatenate(
         [
@@ -217,24 +239,33 @@
     own_head = iota(wide, 0) // PROPS == iota(wide, 1) // DH
     mask = jnp.where(own_head, 0.125, 0.0).astype(BF16)
     spread = jnp.concatenate([query] * HEADS, axis=0) * mask
-    scores = dot_nt(spread, key_ref[s])
+    return dot_nt(spread, key_ref[s])
+
+
+def weigh_sequence(s, scores, base, gate_ref, weights_ref):
+    kv = lax.axis_index("kv")
     gate = gate_ref[s]
-    edge_hit = iota((HEADS, BLOCK), 1) + kv * BLOCK == base - 1
+    edge_hit = (iota((HEADS, BLOCK), 1) + (kv * BLOCK + 1)).astype(F32) == base
     edge = jnp.sum(jnp.where(edge_hit, gate, 0.0), axis=1, keepdims=True)
     gates = jnp.concatenate(
         [jnp.broadcast_to(gate[h : h + 1], (PROPS, BLOCK)) for h in range(HEADS)], axis=0
     )
-    position = iota((HEADS * PROPS, BLOCK), 1) + kv * BLOCK
+    position = (iota((HEADS * PROPS, BLOCK), 1) + kv * BLOCK).astype(F32)
     live = position < base
     scores = jnp.where(live, scores - gates, MASKED)
     peak = jnp.max(scores, axis=1, keepdims=True)
     weights = jnp.where(live, jnp.exp(scores - peak), 0.0)
     total = jnp.sum(weights, axis=1, keepdims=True)
-    weighted = dot_nn(weights.astype(BF16), value_ref[s])
+    weights_ref[s] = weights.astype(BF16)
     some = total > 0.0
     safe = jnp.where(some, total, 1.0)
-    weighted = weighted * (1.0 / safe)
     log_sum = jnp.where(some, peak + jnp.log(safe), MASKED)
+    return 1.0 / safe, log_sum, edge
+
+
+def send_sequence(s, weighted, scale, log_sum, edge, tail, out_ref):
+    peer = s * 2 * QUARTERS
+    weighted = weighted * scale
     lane = iota((PROPS, WIDTH), 1) // DH
     joined = jnp.zeros((PROPS, WIDTH), F32)
     for h in range(HEADS):
@@ -247,17 +278,20 @@
         second = slice((2 * c + 1) * PROPS, (2 * c + 2) * PROPS)
         sums = pieces(jnp.where(even, log_sum[first], log_sum[second]))
         edges = pieces(jnp.where(even, edge[2 * c : 2 * c + 1], edge[2 * c + 1 : 2 * c + 2]))
-        extra = jnp.zeros((PROPS, LANES), F32)
+        extra = jnp.concatenate([tail, tail], axis=0)
         for i, piece in enumerate(sums + edges):
             extra = jnp.where(slot == i, piece, extra)
         part = joined[:, LANES * c : LANES * c + LANES]
+        high = part.astype(BF16).astype(F32)
+        low = part - high
         for e in range(2):
+            rows = slice(SUB * e, SUB * e + SUB)
             out_ref[peer + e * QUARTERS + c] = jnp.concatenate(
-                [part[SUB * e : SUB * e + SUB], extra[SUB * e : SUB * e + SUB]], axis=0
+                [high[rows], low[rows], extra[rows]], axis=0
             ).astype(BF16)
 
 
-def tree_kernel(parents_ref, gate_ref, got_ref, out_ref, gates_ref):
+def attend_tree(parents_ref, gate_ref, got_ref, out_ref):
     kv = lax.axis_index("kv")
     group = lax.div(kv, QUARTERS)
     quarter = lax.rem(kv, QUARTERS)
@@ -299,12 +333,6 @@
     log_sum = peak + jnp.log(total)
     out_ref[0:SUB] = jnp.where(left, weighted[:SUB], weighted[SUB:])
     out_ref[SUB:] = jnp.where(left, log_sum[:SUB], log_sum[SUB:])
-    for c in range(QUARTERS):
-        gate = jnp.sum(got_ref[c, 24:32].astype(F32), axis=0, keepdims=True)
-        for j in range(2):
-            for t in range(SEQS):
-                at = DH * j + PROPS * t
-                gates_ref[t, 2 * c + j : 2 * c + j + 1, :] = gate[:, at : at + PROPS]
 
 
 def merge_kernel(got_ref, tree_ref, consts_ref, out_ref):
@@ -315,7 +343,7 @@
     slot = source // 2
     sums_of = jnp.where(mine & (slot < 3), 1.0, 0.0).astype(BF16)
     edges_of = jnp.where(mine & (slot >= 3) & (slot < 6), 1.0, 0.0).astype(BF16)
-    extra = got_ref[:, SUB:, :].reshape(N_KV * SUB, LANES)
+    extra = got_ref[:, 2 * SUB :, :].reshape(N_KV * SUB, LANES)
     log_sums = dot_nn(extra, sums_of)
     edges = dot_nn(extra, edges_of)
     edge = edges[0:SUB]
@@ -331,11 +359,13 @@
     for p in range(N_KV):
         weight = jnp.exp(log_sums[SUB * p : SUB * p + SUB] - top)
         below = below + weight
-        above = above + weight * got_ref[p, 0:SUB].astype(F32)
+        part = got_ref[p, 0:SUB].astype(F32) + got_ref[p, SUB : 2 * SUB].astype(F32)
+        above = above + weight * part
     attended = above / below
-    normed = (attended * head_scale(attended) * consts_ref[2:3]).astype(BF16)
+    normed = attended * head_scale(attended) * consts_ref[2:3]
+    whole = normed.astype(BF16)
     for p in range(N_KV):
-        out_ref[p] = normed
+        out_ref[p] = whole
 
 
 def out_kernel(got_ref, w_ref, out_ref):
@@ -349,23 +379,51 @@
 
 
 def write_kernel(
-    lengths_ref, accepted_ref, got_ref, key_ref, value_ref, _k, _v, new_key_hbm, new_value_hbm, rows_ref, sems
+    lengths_ref, accepted_ref, parts_ref, got_ref, key_hbm, value_hbm, _k, _v,
+    new_key_hbm, new_value_hbm, gates_ref, old_ref, rows_ref, sems,
 ):
     kv = lax.axis_index("kv")
     window = 2 * PROPS
+    firsts = [lengths_ref[s] + accepted_ref[s] - kv * BLOCK for s in range(SEQS)]
+    mine = [(first > -PROPS) & (first < BLOCK) for first in firsts]
+    starts = [
+        pl.multiple_of(jnp.minimum(lax.div(jnp.maximum(first, 0), PROPS) * PROPS, BLOCK - window), PROPS)
+        for first in firsts
+    ]
+
+    def load(s, i):
+        source = (key_hbm, value_hbm)[i].at[s, pl.ds(starts[s], window), :]
+        return pltpu.make_async_copy(source, old_ref.at[2 * s + i], sems.at[0, 2 * s + i])
+
+    def store(s, i):
+        target = (new_key_hbm, new_value_hbm)[i].at[s, pl.ds(starts[s], window), :]
+        return pltpu.make_async_copy(rows_ref.at[2 * s + i], target, sems.at[1, 2 * s + i])
+
     for s in range(SEQS):
-        first = lengths_ref[s] + accepted_ref[s] - kv * BLOCK
-
-        @pl.when((first > -PROPS) & (first < BLOCK))
+
+        @pl.when(mine[s])
         def _():
-            start = jnp.minimum(lax.div(jnp.maximum(first, 0), PROPS) * PROPS, BLOCK - window)
-            start = pl.multiple_of(start, PROPS)
-            slot = iota((window, PROPS), 0) + start - first
-            placing = (slot == iota((window, PROPS), 1)).astype(F32).astype(BF16)
-            line = iota((window, WIDTH), 0) + start - first
+            for i in range(2):
+                load(s, i).start()
+
+    for c in range(QUARTERS):
+        extra = parts_ref[c, 2 * SUB : 3 * SUB].astype(F32)
+        gate = extra[:, PROPS : 2 * PROPS]
+        for i in (2, 3):
+            gate = gate + extra[:, PROPS * i : PROPS * (i + 1)]
+        for j in range(2):
+            for t in range(SEQS):
+                at = SEQS * j + t
+                gates_ref[t, 2 * c + j : 2 * c + j + 1, :] = gate[at : at + 1]
+    for s in range(SEQS):
+
+        @pl.when(mine[s])
+        def _():
+            offset = starts[s] - firsts[s]
+            placing = (iota((window, PROPS), 0) + offset == iota((window, PROPS), 1)).astype(F32).astype(BF16)
+            line = iota((window, WIDTH), 0) + offset
             hit = (line >= 0) & (line < PROPS)
-            copies = []
-            for i, (old_ref, new_hbm) in enumerate(((key_ref, new_key_hbm), (value_ref, new_value_hbm))):
+            for i in range(2):
                 at = SUB * (i + 1)
                 rows = jnp.concatenate(
                     [
@@ -381,17 +439,17 @@
                     axis=1,
                 )
                 written = dot_nn(placing, rows)
-                old = old_ref[s, pl.ds(start, window), :].astype(F32)
+                load(s, i).wait()
+                old = old_ref[2 * s + i].astype(F32)
                 rows_ref[2 * s + i] = jnp.where(hit, written, old).astype(BF16)
-                copies.append(
-                    pltpu.make_async_copy(
-                        rows_ref.at[2 * s + i], new_hbm.at[s, pl.ds(start, window), :], sems.at[i]
-                    )
-                )
-            for copy in copies:
-                copy.start()
-            for copy in copies:
-                copy.wait()
+                store(s, i).start()
+
+    for s in range(SEQS):
+
+        @pl.when(mine[s])
+        def _():
+            for i in range(2):
+                store(s, i).wait()
 
 
 def exchange(array):
@@ -430,7 +488,7 @@
             jax.ShapeDtypeStruct((N_KV * SEND_A, LANES), F32),
             jax.ShapeDtypeStruct((SUB, LANES), F32),
         ),
-        in_specs=[hbm()] * 10,
+        in_specs=[hbm()] * 12,
         out_specs=(vmem(), vmem()),
         scratch_shapes=[
             pltpu.VMEM((SEQS, PROPS, DH), BF16),
@@ -443,7 +501,9 @@
             pltpu.VMEM((1, DH), F32),
             pltpu.VMEM((1, DH), F32),
             pltpu.VMEM((1, 2 * HEADS), F32),
-            pltpu.SemaphoreType.DMA((10,)),
+            pltpu.VMEM((1, SEQS), jnp.int32),
+            pltpu.VMEM((1, SEQS), jnp.int32),
+            pltpu.SemaphoreType.DMA((12,)),
         ],
         cost_estimate=cost(13_000_000, 700_000),
         compiler_params=limit(8),
@@ -454,30 +514,11 @@
             (
                 tokens, line(norm_gain), w_query, w_key, w_value, w_forget.T,
                 line(query_gain), line(key_gain), line(head_gain), forget_bias.reshape(1, 2 * HEADS),
+                lengths.reshape(1, SEQS), accepted.reshape(1, SEQS),
             ),
         )
     )
     got = exchange(sent.reshape(N_KV, 1, SEND_A * LANES)).reshape(N_KV * SEND_A, LANES)
-    consts, key_cache, value_cache, gate_cache = lax.optimization_barrier(
-        (consts, key_cache, value_cache, gate_cache)
-    )
-    keys, values, gate_block, new_keys, new_values = pl.pallas_call(
-        stage_kernel,
-        out_shape=(
-            pltpu.VMEM(key_cache.shape, BF16),
-            pltpu.VMEM(value_cache.shape, BF16),
-            jax.ShapeDtypeStruct(gate_cache.shape, F32),
-            pltpu.HBM(key_cache.shape, BF16),
-            pltpu.HBM(value_cache.shape, BF16),
-        ),
-        in_specs=[hbm()] * 3,
-        out_specs=(vmem(), vmem(), vmem(), hbm(), hbm()),
-        scratch_shapes=[pltpu.SemaphoreType.DMA((5, SEQS))],
-        cost_estimate=cost(500_000_000, 8_500_000),
-        compiler_params=limit(8),
-        name="stage",
-    )(stay(key_cache), stay(value_cache), stay(gate_cache))
-    got, keys, values = lax.optimization_barrier((got, keys, values))
     sent, gate_row = pl.pallas_call(
         finish_kernel,
         out_shape=(
@@ -491,43 +532,47 @@
         name="finish",
     )(got, consts)
     rows = exchange(sent)
-    sent = pl.pallas_call(
+    gate_row, key_cache, value_cache, gate_cache = lax.optimization_barrier(
+        (gate_row, key_cache, value_cache, gate_cache)
+    )
+    keys, held, gate_block, new_keys, new_values = pl.pallas_call(
+        stage_kernel,
+        out_shape=(
+            cache,
+            jax.ShapeDtypeStruct((HELD, BLOCK, WIDTH), BF16),
+            jax.ShapeDtypeStruct(gate_cache.shape, F32),
+            pltpu.HBM(key_cache.shape, BF16),
+            pltpu.HBM(value_cache.shape, BF16),
+        ),
+        in_specs=[hbm()] * 3,
+        out_specs=(vmem(), vmem(), vmem(), hbm(), hbm()),
+        scratch_shapes=[
+            pltpu.VMEM((SEQS - HELD, BLOCK, WIDTH), BF16),
+            pltpu.SemaphoreType.DMA((3, 2 * SEQS)),
+        ],
+        cost_estimate=cost(500_000_000, 8_500_000),
+        compiler_params=limit(8),
+        name="stage",
+    )(stay(key_cache), stay(value_cache), stay(gate_cache))
+    rows, keys, held, gate_block = lax.optimization_barrier((rows, keys, held, gate_block))
+    sent, tree = pl.pallas_call(
         attend_kernel,
-        out_shape=jax.ShapeDtypeStruct((N_KV, SEND_C, LANES), BF16),
-        in_specs=[smem(), smem()] + [vmem()] * 4,
-        out_specs=vmem(),
+        out_shape=(
+            jax.ShapeDtypeStruct((N_KV, SEND_C, LANES), BF16),
+            jax.ShapeDtypeStruct((2 * SUB, LANES), F32),
+        ),
+        in_specs=[vmem()] * 7 + [hbm()],
+        out_specs=(vmem(), vmem()),
+        scratch_shapes=[
+            pltpu.VMEM((SEQS - HELD, BLOCK, WIDTH), BF16),
+            pltpu.VMEM((SEQS, HEADS * PROPS, BLOCK), BF16),
+            pltpu.SemaphoreType.DMA((SEQS + 1,)),
+        ],
         cost_estimate=cost(600_000_000, 4_500_000),
         compiler_params=limit(16),
         name="attend",
-    )(lengths, accepted, rows, close(keys), close(values), gate_block)
-    got = exchange(sent)
-    tree, gates = pl.pallas_call(
-        tree_kernel,
-        out_shape=(
-            jax.ShapeDtypeStruct((2 * SUB, LANES), F32),
-            jax.ShapeDtypeStruct((SEQS, HEADS, PROPS), F32),
-        ),
-        in_specs=[vmem()] * 3,
-        out_specs=(vmem(), vmem()),
-        cost_estimate=cost(2_000_000, 300_000),
-        compiler_params=limit(8),
-        name="tree",
-    )(parents, gate_row, rows)
-    new_keys, new_values = pl.pallas_call(
-        write_kernel,
-        out_shape=(cache, cache),
-        in_specs=[smem(), smem(), vmem(), vmem(), vmem(), hbm(), hbm()],
-        out_specs=(hbm(), hbm()),
-        scratch_shapes=[
-            pltpu.VMEM((2 * SEQS, 2 * PROPS, WIDTH), BF16),
-            pltpu.SemaphoreType.DMA((2,)),
-        ],
-        input_output_aliases={5: 0, 6: 1},
-        cost_estimate=cost(60_000_000, 8_500_000),
-        compiler_params=limit(8),
-        name="write",
-    )(lengths, accepted, rows, close(keys), close(values), stay(new_keys), stay(new_values))
-    tree, new_keys, new_values = lax.optimization_barrier((tree, new_keys, new_values))
+    )(consts, gate_row, parents, rows, keys, held, gate_block, stay(value_cache))
+    parts = exchange(sent)
     sent = pl.pallas_call(
         merge_kernel,
         out_shape=jax.ShapeDtypeStruct((N_KV, SUB, LANES), BF16),
@@ -536,8 +581,8 @@
         cost_estimate=cost(8_000_000, 200_000),
         compiler_params=limit(8),
         name="merge",
-    )(got, tree, consts)
-    got = exchange(sent)
+    )(parts, tree, consts)
+    normed = exchange(sent)
     term = pl.pallas_call(
         out_kernel,
         out_shape=jax.ShapeDtypeStruct((ROWS, DH), BF16),
@@ -546,8 +591,26 @@
         cost_estimate=cost(4_000_000, 150_000),
         compiler_params=limit(8),
         name="out",
-    )(got, w_out.T)
+    )(normed, w_out.T)
     other = lax.ppermute(term, "tp", [(0, 1), (1, 0)])
+    term, parts = lax.optimization_barrier((term, parts))
+    new_keys, new_values, gates = pl.pallas_call(
+        write_kernel,
+        out_shape=(cache, cache, jax.ShapeDtypeStruct((SEQS, HEADS, PROPS), F32)),
+        in_specs=[smem(), smem(), vmem(), vmem()] + [hbm()] * 4,
+        out_specs=(hbm(), hbm(), vmem()),
+        scratch_shapes=[
+            pltpu.VMEM((2 * SEQS, 2 * PROPS, WIDTH), BF16),
+            pltpu.VMEM((2 * SEQS, 2 * PROPS, WIDTH), BF16),
+            pltpu.SemaphoreType.DMA((2, 2 * SEQS)),
+        ],
+        input_output_aliases={6: 0, 7: 1},
+        cost_estimate=cost(60_000_000, 1_000_000),
+        compiler_params=limit(8),
+        name="write",
+    )(
+        lengths, accepted, parts, rows, stay(key_cache), stay(value_cache), stay(new_keys), stay(new_values)
+    )
     layer_out = (term.astype(F32) + other.astype(F32)).astype(BF16)
     return (layer_out.reshape(SEQS, PROPS, DH), new_keys, new_values, gates.transpose(0, 2, 1))
 

time: 82.9 us -> 80.7 us (0.973)
  blocking collectives: 28 us -> 51.1 us
  starting transfers between devices: 21.8 us -> 10.8 us
  waiting for transfers between devices: 15.5 us -> 6.21 us
  local copies, waits for them, and re-layouts: 4.53 us -> 0.02 us
    all_to_all x2 -> x3, blocking collectives: 28 us -> 51.1 us  [exchange(): return lax.all_to_all(array, 'kv', split_axis=0, concat_axis=0, tiled=True)]
    all_to_all x2 -> x1, starting transfers between devices: 17 us -> 5.66 us  [exchange(): return lax.all_to_all(array, 'kv', split_axis=0, concat_axis=0, tiled=True)]
    all_to_all x2 -> x1, waiting for transfers between devices: 14.6 us -> 6.21 us  [exchange(): return lax.all_to_all(array, 'kv', split_axis=0, concat_axis=0, tiled=True)]
    unnamed x14 -> x8, local copies, waits for them, and re-layouts: 4.53 us -> 0.02 us
    ppermute x1, waiting for transfers between devices: 0.84 us -> 0.01 us  [shards(): other = lax.ppermute(term, 'tp', [(0, 1), (1, 0)])]
    pallas_call x4 -> x3, Pallas kernels: 8.67 us -> 8.17 us  [the longest x1 3.69 us: shards(): pl.pallas_call(stage_kernel, out_shape=(cache, jax.ShapeDtypeStruct((HELD...]
  transfers between devices with their start and end apart: 3 -> 2, of which waited for: 3 -> 1; matrix products, arithmetic and copies ran while one was open for 0% -> 0% of each run, Pallas kernels for 7% -> 6%
where the time goes in v2:
time: 80.7 us; the launch traced here: 80.3 us
  blocking collectives  51.1 us (63%)
  Pallas kernels  10.8 us (13%)
  starting transfers between devices  10.8 us (13%)
  waiting for transfers between devices  6.21 us (8%)
    all_to_all x3, blocking collectives, exchange(): return lax.all_to_all(array, 'kv', split_axis=0, concat_axis=0, tiled=True)  51.1 us
    all_to_all x1, waiting for transfers between devices, exchange(): return lax.all_to_all(array, 'kv', split_axis=0, concat_axis=0, tiled=True)  6.21 us
    all_to_all x1, starting transfers between devices, exchange(): return lax.all_to_all(array, 'kv', split_axis=0, concat_axis=0, tiled=True)  5.66 us
    ppermute x1, starting transfers between devices, shards(): other = lax.ppermute(term, 'tp', [(0, 1), (1, 0)])  5.15 us
    pallas_call x1, Pallas kernels, shards(): pl.pallas_call(stage_kernel, out_shape=(cache, jax.ShapeDtypeStruct((HELD...  3.69 us
    pallas_call x1, Pallas kernels, shards(): pl.pallas_call(attend_kernel, out_shape=(jax.ShapeDtypeStruct((N_KV, SEND...  3.04 us
  transfers between devices with their start and end apart: 2, of which 1 were waited for; matrix products, arithmetic and copies ran while one was open for 0% of the time, Pallas kernels for 6%

profile of v2, /device:TPU:1, one launch (start us, length us, event | category | flops | bytes accessed | tf_op | source)
XLA Modules:
  0.0 80.3 jit_solution(16565936775943564445)
XLA Ops:
  0.6 1.3 %project.1 = (f32[832,128]{1,0:T(8,128)S(1)}, f32[8,128]{1,0:T(8,128)S(1)}) custom-call(bf16[4,16,64]{2,1,0:T(8,128)(2,1)} %x_hbm.1, f32[1,64]{1,0:T(1,128)} %bitcast.20, bf16[64,512]{1,0:T(8,128)(2,1)} %wq_hbm.1, bf16[64,512]{1,0:T(8,128)(2,1)} %wk_hbm.1, bf16[64,512]{1,0:T(8,128)(2,1)} %wv_hbm.1, bf16[16,2048]{1,0:T(8,128)(2,1)} %bitcast.18, ...), custom_call_target="tpu_custom_call" | custom-call | flops 13000000 | bytes 700000 | tf_op jit(solution)/shard_map/project/pallas_call | solution.py:485
  2.0 25.5 %all_to_all.20 = f32[32,1,3328]{2,1,0:T(1,128)S(1)} all-to-all(f32[32,1,3328]{2,1,0:T(1,128)S(1)} %bitcast.14), channel_id=1, replica_groups=mesh['dp'=4,'kv'=32,'tp'=2] {'kv'}, dimensions={0} | all-to-all | bytes 851968 | tf_op jit(solution)/shard_map/all_to_all | solution.py:456
  27.5 0.9 %finish.1 = (bf16[32,24,128]{2,1,0:T(8,128)(2,1)}, f32[1,128]{1,0:T(1,128)S(1)}) custom-call(f32[832,128]{1,0:T(8,128)S(1)} %bitcast.13, f32[8,128]{1,0:T(8,128)S(1)} %get-tuple-element.28.consts_ref), custom_call_target="tpu_custom_call" | custom-call | flops 1000000 | bytes 700000 | tf_op jit(solution)/shard_map/finish/pallas_call | solution.py:522
  28.4 5.7 %all-to-all-start.1 = ((bf16[32,24,128]{2,1,0:T(8,128)(2,1)}), bf16[32,24,128]{2,1,0:T(8,128)(2,1)S(1)}, u32[]{:S(2)}, u32[]{:S(2)}) async-start(bf16[32,24,128]{2,1,0:T(8,128)(2,1)} %get-tuple-element.32), calls=%async_computation.1 | async-start | bytes 393216 | tf_op jit(solution)/shard_map/all_to_all | solution.py:456
  34.1 0.0 copy-start.1
  34.1 3.7 %stage.1 = (bf16[4,512,512]{2,1,0:T(8,128)(2,1)S(1)}, bf16[2,512,512]{2,1,0:T(8,128)(2,1)S(1)}, f32[4,8,512]{2,1,0:T(8,128)S(1)}, bf16[4,512,512]{2,1,0:T(8,128)(2,1)}, bf16[4,512,512]{2,1,0:T(8,128)(2,1)}) custom-call(bf16[4,512,512]{2,1,0:T(8,128)(2,1)} %key_hbm.1, bf16[4,512,512]{2,1,0:T(8,128)(2,1)} %value_hbm.2, f32[4,8,512]{2,1,0:T(8,128)} %gate_hbm), custom_call_target="tpu_custom_call" | custom-call | flops 500000000 | bytes 8500000 | tf_op jit(solution)/shard_map/stage/pallas_call | solution.py:538
  37.8 6.2 %all-to-all-done.1.got_ref = bf16[32,24,128]{2,1,0:T(8,128)(2,1)S(1)} async-done(((bf16[32,24,128]{2,1,0:T(8,128)(2,1)}), bf16[32,24,128]{2,1,0:T(8,128)(2,1)S(1)}, u32[]{:S(2)}, u32[]{:S(2)}) %all-to-all-start.1) | async-done | bytes 196640 | tf_op jit(solution)/shard_map/all_to_all | solution.py:456
  44.0 0.0 copy-done.1
  44.0 0.0 copy-start
  44.0 0.0 copy-start.2
  44.0 0.0 copy-start.3
  44.0 3.0 %attend.1 = (bf16[32,24,128]{2,1,0:T(8,128)(2,1)S(1)}, f32[16,128]{1,0:T(8,128)S(1)}) custom-call(f32[8,128]{1,0:T(8,128)S(1)} %get-tuple-element.28.consts_ref, f32[1,128]{1,0:T(1,128)S(1)} %get-tuple-element.31.row_ref, s32[4,16]{1,0:T(4,128)S(1)} %copy-done.1, bf16[32,24,128]{2,1,0:T(8,128)(2,1)S(1)} %all-to-all-done.1.got_ref, ...), custom_call_target="tpu_custom_call" | custom-call | flops 600000000 | bytes 4500000 | tf_op jit(solution)/shard_map/attend/pallas_call | solution.py:558
  47.0 13.4 %all_to_all.21.got_ref.parts_ref = bf16[32,24,128]{2,1,0:T(8,128)(2,1)S(1)} all-to-all(bf16[32,24,128]{2,1,0:T(8,128)(2,1)S(1)} %get-tuple-element.43), channel_id=1, replica_groups=mesh['dp'=4,'kv'=32,'tp'=2] {'kv'}, dimensions={0} | all-to-all | bytes 393216 | tf_op jit(solution)/shard_map/all_to_all | solution.py:456
  60.4 0.3 merge.1
  60.7 12.2 %all_to_all.22.got_ref = bf16[32,8,128]{2,1,0:T(8,128)(2,1)S(1)} all-to-all(bf16[32,8,128]{2,1,0:T(8,128)(2,1)S(1)} %merge.1), channel_id=1, replica_groups=mesh['dp'=4,'kv'=32,'tp'=2] {'kv'}, dimensions={0} | all-to-all | bytes 131072 | tf_op jit(solution)/shard_map/all_to_all | solution.py:456
  72.9 0.0 copy-done
  72.9 0.1 out.1
  73.1 5.2 %collective-permute-start = (bf16[64,64]{1,0:T(8,128)(2,1)S(1)}, bf16[64,64]{1,0:T(8,128)(2,1)S(1)}, u32[]{:S(2)}, u32[]{:S(2)}) collective-permute-start(bf16[64,64]{1,0:T(8,128)(2,1)S(1)} %out.1), channel_id=1, source_target_pairs={{0,1},{1,0},{2,3},{3,2},{4,5},{5,4},{6,7},{7,6},{8,9},{9,8},{10,11... | collective-permute-start | bytes 24584 | tf_op jit(solution)/shard_map/ppermute | solution.py:595
  78.2 0.0 copy-done.2
  78.2 0.0 copy-done.3
  78.2 1.4 %write.1 = (bf16[4,512,512]{2,1,0:T(8,128)(2,1)}, bf16[4,512,512]{2,1,0:T(8,128)(2,1)}, f32[4,8,16]{2,1,0:T(8,128)}) custom-call(s32[4]{0:T(128)S(1)} %copy-done.2, s32[4]{0:T(128)S(1)} %copy-done.3, bf16[32,24,128]{2,1,0:T(8,128)(2,1)S(1)} %all_to_all.21.got_ref.parts_ref, ...), custom_call_target="tpu_custom_call", output_to_operand_aliasing={{0}: (6, {}), {1}: (7, {})} | custom-call | flops 60000000 | bytes 1000000 | tf_op jit(solution)/shard_map/write/pallas_call | solution.py:597
  79.7 0.0 collective-permute-done
  79.7 0.6 add_convert_fusion
Async XLA Ops:
  28.4 15.6 %all-to-all-start.1 = ((bf16[32,24,128]{2,1,0:T(8,128)(2,1)}), bf16[32,24,128]{2,1,0:T(8,128)(2,1)S(1)}, u32[]{:S(2)}, u32[]{:S(2)}) async-start(bf16[32,24,128]{2,1,0:T(8,128)(2,1)} %get-tuple-element.32), calls=%async_computation.1 | async-start | bytes 393216 | tf_op jit(solution)/shard_map/all_to_all | solution.py:456
  34.1 9.9 %copy-start.1 = (s32[4,16]{1,0:T(4,128)S(1)}, s32[4,16]{1,0:T(4,128)}, u32[]{:S(2)}) copy-start(s32[4,16]{1,0:T(4,128)} %parents_ref.1) | copy-start | bytes 772
  44.0 29.0 %copy-start = (bf16[512,64]{0,1:T(8,128)(2,1)S(1)}, bf16[512,64]{0,1:T(8,128)(2,1)}, u32[]{:S(2)}) copy-start(bf16[512,64]{0,1:T(8,128)(2,1)} %param.27) | copy-start | bytes 196612
  44.0 34.2 %copy-start.2 = (s32[4]{0:T(128)S(1)}, s32[4]{0:T(128)}, u32[]{:S(2)}) copy-start(s32[4]{0:T(128)} %lengths_ref.1) | copy-start | bytes 52
  44.0 34.2 %copy-start.3 = (s32[4]{0:T(128)S(1)}, s32[4]{0:T(128)}, u32[]{:S(2)}) copy-start(s32[4]{0:T(128)} %accepted_ref.1) | copy-start | bytes 52
  73.1 6.6 %collective-permute-start = (bf16[64,64]{1,0:T(8,128)(2,1)S(1)}, bf16[64,64]{1,0:T(8,128)(2,1)S(1)}, u32[]{:S(2)}, u32[]{:S(2)}) collective-permute-start(bf16[64,64]{1,0:T(8,128)(2,1)S(1)} %out.1), channel_id=1, source_target_pairs={{0,1},{1,0},{2,3},{3,2},{4,5},{5,4},{6,7},{7,6},{8,9},{9,8},{10,11... | collective-permute-start | bytes 24584 | tf_op jit(solution)/shard_map/ppermute | solution.py:595

commit v3 on v2

v3 whole, which is shorter than its diff:
```python
import jax
import jax.numpy as jnp
from jax import lax
from jax.experimental import pallas as pl
from jax.experimental.pallas import tpu as pltpu
from jax.sharding import PartitionSpec as P

EPSILON = 1e-06
MASKED = -1e30
F32 = jnp.float32
BF16 = jnp.bfloat16

LANES = 128
SUB = 8
N_KV = 32
QUARTERS = 4
ROWS = 64
HEADS = 8
DH = 64
WIDTH = 512
PROPS = 16
SEQS = 4
BLOCK = 512
SEND_A = 9
SEND_KV = 24
SEND_B = SUB + SEND_KV
SEND_C = 9
SEND_D = 24
HELD = 2


def iota(shape, dim):
    return lax.broadcasted_iota(jnp.int32, shape, dim)


def dot_nn(a, b):
    return lax.dot_general(a, b, (((1,), (0,)), ((), ())), preferred_element_type=F32)


def dot_nt(a, b):
    return lax.dot_general(a, b, (((1,), (1,)), ((), ())), preferred_element_type=F32)


def pieces(x):
    high = x.astype(BF16).astype(F32)
    rest = x - high
    middle = rest.astype(BF16).astype(F32)
    return high, middle, rest - middle


def left_of(shape):
    return iota(shape, len(shape) - 1) < DH


def swapped(block):
    return pltpu.roll(block, DH, 1)


def packed(top, bottom):
    left = left_of(top.shape)
    return jnp.where(left, top, swapped(bottom)), jnp.where(left, swapped(top), bottom)


def unpacked_rows(read, s):
    tiles = []
    for c in range(QUARTERS):
        even, odd = (read(s * HEADS + 2 * c + j).astype(F32) for j in range(2))
        tiles.append(jnp.concatenate(packed(even, odd), axis=0))
    return jnp.concatenate(tiles, axis=1).astype(BF16)


def vmem():
    return pl.BlockSpec(memory_space=pltpu.VMEM)


def stay(array):
    return pltpu.with_memory_space_constraint(array, pltpu.HBM)


def hbm():
    return pl.BlockSpec(memory_space=pltpu.HBM)


def cost(flops, moved):
    return pl.CostEstimate(flops=flops, bytes_accessed=moved, transcendentals=0)


def doubled(gain_ref):
    gain = gain_ref[...]
    return jnp.concatenate([gain, gain], axis=1)


def project_kernel(
    x_hbm, gain_hbm, wq_hbm, wk_hbm, wv_hbm, wf_hbm, qgain_hbm, kgain_hbm, hgain_hbm, bias_hbm, lengths_hbm, accepted_hbm,
    out_ref, part_ref, consts_ref,
    x_ref, gain_ref, wq_ref, wk_ref, wv_ref, wf_ref, qgain_ref, kgain_ref, hgain_ref, bias_ref, lengths_ref, accepted_ref, sems,
):
    kv = lax.axis_index("kv")
    tp = lax.axis_index("tp")
    column = pl.multiple_of(lax.div(kv, 2) * LANES, LANES)
    pairs = (
        (x_hbm, x_ref),
        (gain_hbm, gain_ref),
        (wq_hbm, wq_ref),
        (wk_hbm, wk_ref),
        (wv_hbm, wv_ref),
        (wf_hbm.at[:, pl.ds(column, LANES)], wf_ref),
        (qgain_hbm, qgain_ref),
        (kgain_hbm, kgain_ref),
        (hgain_hbm, hgain_ref),
        (bias_hbm, bias_ref),
        (lengths_hbm, lengths_ref),
        (accepted_hbm, accepted_ref),
    )
    copies = [pltpu.make_async_copy(a, b, sems.at[n]) for n, (a, b) in enumerate(pairs)]
    for copy in copies:
        copy.start()
    for copy in copies:
        copy.wait()
    at = tp * HEADS + lax.rem(kv, HEADS)
    spot = iota((1, 2 * HEADS), 1)
    bias = jnp.sum(jnp.where(spot == at, bias_ref[...], 0.0), axis=1, keepdims=True)
    consts_ref[0:1] = doubled(qgain_ref)
    consts_ref[1:2] = doubled(kgain_ref)
    consts_ref[2:3] = doubled(hgain_ref)
    consts_ref[3:4] = jnp.broadcast_to(bias, (1, LANES))
    consts_ref[4:5, 0:SEQS] = (lengths_ref[...] + accepted_ref[...]).astype(F32)
    x = x_ref[...].reshape(ROWS, DH).astype(F32)
    scaled = (x * gain_ref[...]).astype(BF16)
    blocks = [dot_nn(scaled, w[...]) for w in (wq_ref, wk_ref, wv_ref)]
    wide = jnp.concatenate([scaled, scaled], axis=1)
    half = (iota((ROWS, LANES), 1) // DH == lax.rem(kv, 2)).astype(F32).astype(BF16)
    gates = dot_nt(wf_ref[...], wide * half)
    own = jnp.where(tp == 0, gates[:HEADS], gates[HEADS:])
    squares = jnp.sum(x * x, axis=1, keepdims=True)
    diagonal = iota((ROWS, LANES), 0) == iota((ROWS, LANES), 1)
    square_row = jnp.sum(jnp.where(diagonal, squares, 0.0), axis=0, keepdims=True)[:, :DH]
    for s in range(SEQS):
        for c in range(QUARTERS):
            query, key, value = (
                packed(
                    *(
                        block[at : at + SUB, LANES * c : LANES * c + LANES]
                        for at in (PROPS * s, PROPS * s + SUB)
                    )
                )
                for block in blocks
            )
            for j in range(2):
                head = 2 * c + j
                peer = s * HEADS + head
                out_ref[SEND_A * peer : SEND_A * peer + SUB, :] = query[j]
                out_ref[SEND_A * peer + SUB : SEND_A * (peer + 1), :] = jnp.concatenate(
                    [own[head : head + 1], square_row], axis=1
                )
                high = key[j].astype(BF16).astype(F32)
                part_ref[peer] = jnp.concatenate([high, key[j] - high, value[j]], axis=0).astype(BF16)


def head_scale(block):
    left = iota(block.shape, 1) < DH
    square = block * block
    first = jnp.sum(jnp.where(left, square, 0.0), axis=1, keepdims=True)
    second = jnp.sum(jnp.where(left, 0.0, square), axis=1, keepdims=True)
    return lax.rsqrt(jnp.where(left, first, second) / DH + EPSILON)


def finish_kernel(got_ref, part_ref, consts_ref, out_ref, row_ref, inverse_ref):
    s = lax.div(lax.axis_index("kv"), HEADS)
    query = got_ref[0:SUB]
    tail = got_ref[SUB:SEND_A]
    for p in range(1, N_KV):
        query = query + got_ref[SEND_A * p : SEND_A * p + SUB]
        tail = tail + got_ref[SEND_A * p + SUB : SEND_A * (p + 1)]
    other = swapped(jnp.broadcast_to(tail, (SUB, LANES)))[0:1]
    left = left_of((1, LANES))
    square = jnp.where(left, other, tail)
    gate_sum = jnp.where(left, tail, other)
    inverse_row = lax.rsqrt(square / (N_KV * DH) + EPSILON)
    lane = iota((SUB, LANES), 1)
    first = iota((SUB, LANES), 0) + s * PROPS
    upper = jnp.sum(jnp.where(lane == first, inverse_row, 0.0), axis=1, keepdims=True)
    lower = jnp.sum(jnp.where(lane == first + SUB, inverse_row, 0.0), axis=1, keepdims=True)
    inverse = jnp.where(left_of((SUB, LANES)), upper, lower)
    inverse_ref[...] = inverse
    query = query * inverse
    query = query * head_scale(query) * consts_ref[0:1]
    logit = gate_sum * inverse_row + consts_ref[3:4]
    small = jnp.exp(-jnp.abs(logit))
    one_more = 1.0 + small
    grown = jnp.where(
        one_more == 1.0, small, jnp.log(one_more) * small / jnp.where(one_more == 1.0, 1.0, one_more - 1.0)
    )
    row_ref[...] = jnp.minimum(logit, 0.0) - grown
    whole = query.astype(BF16)
    for p in range(N_KV):
        out_ref[p, 0:SUB] = whole
        out_ref[p, SUB:SEND_B] = part_ref[p]


def stage_kernel(
    key_hbm, value_hbm, gate_hbm, parents_ref, row_ref,
    key_ref, held_ref, gate_ref, bias_ref, new_key_hbm, new_value_hbm,
    rest_ref, sems,
):
    gate_load = pltpu.make_async_copy(gate_hbm, gate_ref, sems.at[2, 0])
    gate_load.start()
    targets = [key_ref.at[s] for s in range(SEQS)]
    targets += [held_ref.at[s] if s < HELD else rest_ref.at[s - HELD] for s in range(SEQS)]
    sources = [key_hbm.at[s] for s in range(SEQS)] + [value_hbm.at[s] for s in range(SEQS)]
    news = [new_key_hbm.at[s] for s in range(SEQS)] + [new_value_hbm.at[s] for s in range(SEQS)]
    loads = [pltpu.make_async_copy(a, b, sems.at[0, n]) for n, (a, b) in enumerate(zip(sources, targets))]
    stores = [pltpu.make_async_copy(a, b, sems.at[1, n]) for n, (a, b) in enumerate(zip(targets, news))]
    for load in loads:
        load.start()
    bias_ref[...] = tree_bias(parents_ref, row_ref)
    for load, store in zip(loads, stores):
        load.wait()
        store.start()
    gate_load.wait()
    for store in stores:
        store.wait()


def tree_bias(parents_ref, row_ref):
    s = lax.div(lax.axis_index("kv"), HEADS)
    square = (PROPS, PROPS)
    step = (iota(square, 0) == parents_ref[pl.ds(s, 1), :]).astype(F32)
    identity = (iota(square, 0) == iota(square, 1)).astype(F32)
    above = identity + step
    reach = step
    for _ in range(3):
        reach = dot_nn(reach, reach)
        above = above + dot_nn(above, reach)
    wide = (PROPS, LANES)
    wanted = iota(wide, 1) == iota(wide, 0) + s * PROPS
    gate = jnp.sum(jnp.where(wanted, row_ref[...], 0.0), axis=1, keepdims=True)
    path = jnp.sum(above * gate, axis=0, keepdims=True)
    return jnp.where(dot_nt(identity, above) > 0.5, -path, MASKED)


def attend_kernel(
    consts_ref, inverse_ref, row_ref, bias_ref, got_ref, key_ref, held_ref, gate_ref, value_hbm,
    out_ref, tree_ref, own_ref, rest_ref, weights_ref, sems,
):
    loads = {}
    for s in range(HELD, SEQS):
        loads[s] = pltpu.make_async_copy(value_hbm.at[s], rest_ref.at[s - HELD], sems.at[s])
        loads[s].start()
    sums = []
    for s in range(SEQS):
        raw = score_sequence(s, got_ref, key_ref)
        sums.append(weigh_sequence(s, raw, consts_ref[4:5, s : s + 1], gate_ref, weights_ref))
    attend_tree(consts_ref, inverse_ref, bias_ref, got_ref, tree_ref, own_ref)
    tail = row_ref[...]
    for s in range(SEQS):
        if s in loads:
            loads[s].wait()
        values = held_ref[s] if s < HELD else rest_ref[s - HELD]
        send_sequence(s, dot_nn(weights_ref[s], values), *sums[s], tail, out_ref)


def score_sequence(s, got_ref, key_ref):
    query = unpacked_rows(lambda p: got_ref[p, 0:SUB], s)
    wide = (HEADS * PROPS, WIDTH)
    own_head = iota(wide, 0) // PROPS == iota(wide, 1) // DH
    mask = jnp.where(own_head, 0.125, 0.0).astype(BF16)
    spread = jnp.concatenate([query] * HEADS, axis=0) * mask
    return dot_nt(spread, key_ref[s])


def weigh_sequence(s, scores, base, gate_ref, weights_ref):
    kv = lax.axis_index("kv")
    gate = gate_ref[s]
    edge_hit = (iota((HEADS, BLOCK), 1) + (kv * BLOCK + 1)).astype(F32) == base
    edge = jnp.sum(jnp.where(edge_hit, gate, 0.0), axis=1, keepdims=True)
    gates = jnp.concatenate(
        [jnp.broadcast_to(gate[h : h + 1], (PROPS, BLOCK)) for h in range(HEADS)], axis=0
    )
    position = (iota((HEADS * PROPS, BLOCK), 1) + kv * BLOCK).astype(F32)
    live = position < base
    scores = jnp.where(live, scores - gates, MASKED)
    peak = jnp.max(scores, axis=1, keepdims=True)
    weights = jnp.where(live, jnp.exp(scores - peak), 0.0)
    total = jnp.sum(weights, axis=1, keepdims=True)
    weights_ref[s] = weights.astype(BF16)
    some = total > 0.0
    safe = jnp.where(some, total, 1.0)
    log_sum = jnp.where(some, peak + jnp.log(safe), MASKED)
    return 1.0 / safe, log_sum, edge


def send_sequence(s, weighted, scale, log_sum, edge, tail, out_ref):
    weighted = weighted * scale
    lane = iota((PROPS, WIDTH), 1) // DH
    joined = jnp.zeros((PROPS, WIDTH), F32)
    for h in range(HEADS):
        joined = jnp.where(lane == h, weighted[h * PROPS : (h + 1) * PROPS], joined)
    whole = (LANES, LANES)
    spread = jnp.where(iota(whole, 0) == iota(whole, 1), log_sum, 0.0)
    log_row = jnp.sum(spread, axis=0, keepdims=True)
    lane = iota((1, LANES), 1)
    for c in range(QUARTERS):
        part = joined[:, LANES * c : LANES * c + LANES]
        both = packed(part[:SUB], part[SUB:])
        for j in range(2):
            h = 2 * c + j
            at = (s * HEADS + h) * SEND_C
            row = jnp.where(lane // PROPS == h, log_row, edge[h : h + 1])
            row = jnp.where(lane // DH == h // QUARTERS, row, tail)
            out_ref[at : at + SUB, :] = both[j]
            out_ref[at + SUB : at + SEND_C, :] = row


def attend_tree(consts_ref, inverse_ref, bias_ref, got_ref, tree_ref, own_ref):
    key = jnp.zeros((SUB, LANES), F32)
    value = jnp.zeros((SUB, LANES), F32)
    for p in range(N_KV):
        high, low, part = (got_ref[p, SUB * i : SUB * i + SUB].astype(F32) for i in range(1, 4))
        key = key + (high + low)
        value = value + part
    inverse = inverse_ref[...]
    key = key * inverse
    key = (key * head_scale(key) * consts_ref[1:2]).astype(BF16).astype(F32)
    value = (value * inverse).astype(BF16).astype(F32)
    own_ref[...] = jnp.concatenate([key, value], axis=0).astype(BF16)
    query = got_ref[lax.axis_index("kv"), 0:SUB].astype(F32)
    left = left_of((PROPS, LANES))
    query, keys, values = (jnp.concatenate([x, swapped(x)], axis=0) for x in (query, key, value))
    query = jnp.where(left, query, 0.0).astype(BF16)
    bias = bias_ref[...]
    scores = dot_nt(query, keys.astype(BF16)) * 0.125 + bias
    peak = jnp.max(scores, axis=1, keepdims=True)
    weights = jnp.where(bias > 0.5 * MASKED, jnp.exp(scores - peak), 0.0)
    total = jnp.sum(weights, axis=1, keepdims=True)
    weighted = dot_nn(weights.astype(BF16), values.astype(BF16)) / total
    log_sum = peak + jnp.log(total)
    tree_ref[0:SUB] = jnp.where(left[:SUB], weighted[:SUB], swapped(weighted[SUB:]))
    tree_ref[SUB:] = jnp.where(left[:SUB], log_sum[:SUB], log_sum[SUB:])


def merge_kernel(got_ref, tree_ref, own_ref, consts_ref, out_ref):
    h = lax.rem(lax.axis_index("kv"), HEADS)
    shape = (LANES, LANES)
    source = iota(shape, 0)
    same = lax.rem(source, PROPS) // SUB == iota(shape, 1) // DH
    choose = jnp.where((source // PROPS == h) & same, 1.0, 0.0).astype(BF16)
    tile = (SUB, LANES)
    wanted = (iota(tile, 1) // PROPS == h) & (lax.rem(iota(tile, 1), SUB) == iota(tile, 0))
    edge_lane = lax.div(h, QUARTERS) * DH + lax.rem(h + 1, QUARTERS) * PROPS
    rows = [got_ref[SEND_C * p + SUB : SEND_C * (p + 1), :] for p in range(N_KV)]
    edge = rows[0]
    for row in rows[1:]:
        edge = edge + row
    edge = jnp.sum(jnp.where(iota((1, LANES), 1) == edge_lane, edge, 0.0), axis=1, keepdims=True)
    spread = jnp.concatenate([jnp.where(wanted, row, 0.0) for row in rows], axis=0)
    log_sums = jnp.zeros((N_KV * SUB, LANES), F32)
    for piece in pieces(spread):
        log_sums = log_sums + dot_nn(piece.astype(BF16), choose)
    top = log_sums[0:SUB]
    for p in range(1, N_KV):
        top = jnp.maximum(top, log_sums[SUB * p : SUB * p + SUB])
    tree_sum = tree_ref[SUB:] - edge
    top = jnp.maximum(top, tree_sum)
    weight = jnp.exp(tree_sum - top)
    below = weight
    above = weight * tree_ref[0:SUB]
    for p in range(N_KV):
        weight = jnp.exp(log_sums[SUB * p : SUB * p + SUB] - top)
        below = below + weight
        part = got_ref[SEND_C * p : SEND_C * p + SUB, :]
        above = above + weight * part
    attended = above / below
    normed = attended * head_scale(attended) * consts_ref[2:3]
    whole = normed.astype(BF16)
    own = own_ref[...]
    for p in range(N_KV):
        out_ref[p, 0:SUB] = whole
        out_ref[p, SUB:SEND_D] = own


def out_kernel(got_ref, w_ref, out_ref):
    rows = jnp.concatenate([unpacked_rows(lambda p: got_ref[p, 0:SUB], s) for s in range(SEQS)], axis=0)
    result = dot_nt(rows, w_ref[...])
    out_ref[...] = result.astype(BF16)


def write_kernel(
    consts_ref, parts_ref, got_ref, key_hbm, value_hbm, _k, _v,
    new_key_hbm, new_value_hbm, gates_ref, old_ref, rows_ref, sems,
):
    kv = lax.axis_index("kv")
    window = 2 * PROPS
    bases = [jnp.max(consts_ref[4:5, s : s + 1]).astype(jnp.int32) for s in range(SEQS)]
    firsts = [base - kv * BLOCK for base in bases]
    mine = [(first > -PROPS) & (first < BLOCK) for first in firsts]
    starts = [
        pl.multiple_of(jnp.minimum(lax.div(jnp.maximum(first, 0), PROPS) * PROPS, BLOCK - window), PROPS)
        for first in firsts
    ]

    def load(s, i):
        source = (key_hbm, value_hbm)[i].at[s, pl.ds(starts[s], window), :]
        return pltpu.make_async_copy(source, old_ref.at[2 * s + i], sems.at[0, 2 * s + i])

    def store(s, i):
        target = (new_key_hbm, new_value_hbm)[i].at[s, pl.ds(starts[s], window), :]
        return pltpu.make_async_copy(rows_ref.at[2 * s + i], target, sems.at[1, 2 * s + i])

    for s in range(SEQS):

        @pl.when(mine[s])
        def _():
            for i in range(2):
                load(s, i).start()

    for h in range(HEADS):
        row = parts_ref[SEND_C * h + SUB : SEND_C * (h + 1), :]
        row = jnp.where(lax.rem(kv, HEADS) < QUARTERS, row[:, DH:], row[:, :DH])
        for t in range(SEQS):
            at = PROPS * t
            gates_ref[t, h : h + 1, :] = row[:, at : at + PROPS]
    for s in range(SEQS):

        @pl.when(mine[s])
        def _():
            offset = starts[s] - firsts[s]
            placing = (iota((window, PROPS), 0) + offset == iota((window, PROPS), 1)).astype(F32).astype(BF16)
            line = iota((window, WIDTH), 0) + offset
            hit = (line >= 0) & (line < PROPS)
            for i in range(2):
                at = SUB * (i + 1)
                rows = unpacked_rows(lambda p: got_ref[p, at : at + SUB], s)
                written = dot_nn(placing, rows)
                load(s, i).wait()
                old = old_ref[2 * s + i].astype(F32)
                rows_ref[2 * s + i] = jnp.where(hit, written, old).astype(BF16)
                store(s, i).start()

    for s in range(SEQS):

        @pl.when(mine[s])
        def _():
            for i in range(2):
                store(s, i).wait()


def exchange(array):
    return lax.all_to_all(array, "kv", split_axis=0, concat_axis=0, tiled=True)


def shards(
    tokens,
    norm_gain,
    w_query,
    w_key,
    w_value,
    w_forget,
    forget_bias,
    query_gain,
    key_gain,
    head_gain,
    w_out,
    key_cache,
    value_cache,
    gate_cache,
    lengths,
    accepted,
    parents,
):
    def line(gain):
        return gain.reshape(1, DH)

    def limit(size):
        return pltpu.CompilerParams(vmem_limit_bytes=size * 2**20)

    cache = jax.ShapeDtypeStruct(key_cache.shape, BF16)
    sent, part, consts = pl.pallas_call(
        project_kernel,
        out_shape=(
            jax.ShapeDtypeStruct((N_KV * SEND_A, LANES), F32),
            jax.ShapeDtypeStruct((N_KV, SEND_KV, LANES), BF16),
            jax.ShapeDtypeStruct((SUB, LANES), F32),
        ),
        in_specs=[hbm()] * 12,
        out_specs=(vmem(), vmem(), vmem()),
        scratch_shapes=[
            pltpu.VMEM((SEQS, PROPS, DH), BF16),
            pltpu.VMEM((1, DH), F32),
            pltpu.VMEM((DH, WIDTH), BF16),
            pltpu.VMEM((DH, WIDTH), BF16),
            pltpu.VMEM((DH, WIDTH), BF16),
            pltpu.VMEM((2 * HEADS, LANES), BF16),
            pltpu.VMEM((1, DH), F32),
            pltpu.VMEM((1, DH), F32),
            pltpu.VMEM((1, DH), F32),
            pltpu.VMEM((1, 2 * HEADS), F32),
            pltpu.VMEM((1, SEQS), jnp.int32),
            pltpu.VMEM((1, SEQS), jnp.int32),
            pltpu.SemaphoreType.DMA((12,)),
        ],
        cost_estimate=cost(13_000_000, 700_000),
        compiler_params=limit(8),
        name="project",
    )(
        *map(
            stay,
            (
                tokens, line(norm_gain), w_query, w_key, w_value, w_forget.T,
                line(query_gain), line(key_gain), line(head_gain), forget_bias.reshape(1, 2 * HEADS),
                lengths.reshape(1, SEQS), accepted.reshape(1, SEQS),
            ),
        )
    )
    got = exchange(sent.reshape(N_KV, 1, SEND_A * LANES)).reshape(N_KV * SEND_A, LANES)
    sent, gate_row, inverse = pl.pallas_call(
        finish_kernel,
        out_shape=(
            jax.ShapeDtypeStruct((N_KV, SEND_B, LANES), BF16),
            jax.ShapeDtypeStruct((1, LANES), F32),
            jax.ShapeDtypeStruct((SUB, LANES), F32),
        ),
        in_specs=[vmem()] * 3,
        out_specs=(vmem(), vmem(), vmem()),
        cost_estimate=cost(1_000_000, 700_000),
        compiler_params=limit(8),
        name="finish",
    )(got, part, consts)
    rows = exchange(sent)
    gate_row, key_cache, value_cache, gate_cache = lax.optimization_barrier(
        (gate_row, key_cache, value_cache, gate_cache)
    )
    keys, held, gate_block, bias, new_keys, new_values = pl.pallas_call(
        stage_kernel,
        out_shape=(
            cache,
            jax.ShapeDtypeStruct((HELD, BLOCK, WIDTH), BF16),
            jax.ShapeDtypeStruct(gate_cache.shape, F32),
            jax.ShapeDtypeStruct((PROPS, PROPS), F32),
            pltpu.HBM(key_cache.shape, BF16),
            pltpu.HBM(value_cache.shape, BF16),
        ),
        in_specs=[hbm()] * 3 + [vmem()] * 2,
        out_specs=(vmem(),) * 4 + (hbm(), hbm()),
        scratch_shapes=[
            pltpu.VMEM((SEQS - HELD, BLOCK, WIDTH), BF16),
            pltpu.SemaphoreType.DMA((3, 2 * SEQS)),
        ],
        cost_estimate=cost(500_000_000, 8_500_000),
        compiler_params=limit(8),
        name="stage",
    )(stay(key_cache), stay(value_cache), stay(gate_cache), parents, gate_row)
    rows, keys, held, gate_block = lax.optimization_barrier((rows, keys, held, gate_block))
    sent, tree, own = pl.pallas_call(
        attend_kernel,
        out_shape=(
            jax.ShapeDtypeStruct((N_KV * SEND_C, LANES), F32),
            jax.ShapeDtypeStruct((2 * SUB, LANES), F32),
            jax.ShapeDtypeStruct((2 * SUB, LANES), BF16),
        ),
        in_specs=[vmem()] * 8 + [hbm()],
        out_specs=(vmem(), vmem(), vmem()),
        scratch_shapes=[
            pltpu.VMEM((SEQS - HELD, BLOCK, WIDTH), BF16),
            pltpu.VMEM((SEQS, HEADS * PROPS, BLOCK), BF16),
            pltpu.SemaphoreType.DMA((SEQS + 1,)),
        ],
        cost_estimate=cost(600_000_000, 4_500_000),
        compiler_params=limit(16),
        name="attend",
    )(consts, inverse, gate_row, bias, rows, keys, held, gate_block, stay(value_cache))
    parts = exchange(sent.reshape(N_KV, 1, SEND_C * LANES)).reshape(N_KV * SEND_C, LANES)
    sent = pl.pallas_call(
        merge_kernel,
        out_shape=jax.ShapeDtypeStruct((N_KV, SEND_D, LANES), BF16),
        in_specs=[vmem()] * 4,
        out_specs=vmem(),
        cost_estimate=cost(8_000_000, 200_000),
        compiler_params=limit(8),
        name="merge",
    )(parts, tree, own, consts)
    normed = exchange(sent)
    term = pl.pallas_call(
        out_kernel,
        out_shape=jax.ShapeDtypeStruct((ROWS, DH), BF16),
        in_specs=[vmem()] * 2,
        out_specs=vmem(),
        cost_estimate=cost(4_000_000, 150_000),
        compiler_params=limit(8),
        name="out",
    )(normed, w_out.T)
    other = lax.ppermute(term, "tp", [(0, 1), (1, 0)])
    term, parts = lax.optimization_barrier((term, parts))
    new_keys, new_values, gates = pl.pallas_call(
        write_kernel,
        out_shape=(cache, cache, jax.ShapeDtypeStruct((SEQS, HEADS, PROPS), F32)),
        in_specs=[vmem()] * 3 + [hbm()] * 4,
        out_specs=(hbm(), hbm(), vmem()),
        scratch_shapes=[
            pltpu.VMEM((2 * SEQS, 2 * PROPS, WIDTH), BF16),
            pltpu.VMEM((2 * SEQS, 2 * PROPS, WIDTH), BF16),
            pltpu.SemaphoreType.DMA((2, 2 * SEQS)),
        ],
        input_output_aliases={5: 0, 6: 1},
        cost_estimate=cost(60_000_000, 1_000_000),
        compiler_params=limit(8),
        name="write",
    )(
        consts, parts, normed, stay(key_cache), stay(value_cache), stay(new_keys), stay(new_values)
    )
    layer_out = (term.astype(F32) + other.astype(F32)).astype(BF16)
    return (layer_out.reshape(SEQS, PROPS, DH), new_keys, new_values, gates.transpose(0, 2, 1))


def solution(mesh):
    placed = (
        P("dp", None, "kv"),
        P("kv"),
        P("kv", "tp"),
        P("kv", "tp"),
        P("kv", "tp"),
        P(),
        P(),
        P(),
        P(),
        P(),
        P("tp", "kv"),
        P("dp", "kv", "tp"),
        P("dp", "kv", "tp"),
        P("dp", "tp", "kv"),
        P("dp"),
        P("dp"),
        P("dp", None),
    )
    return jax.shard_map(
        shards,
        mesh=mesh,
        in_specs=placed,
        out_specs=(
            P("dp", None, "kv"),
            P("dp", "kv", "tp"),
            P("dp", "kv", "tp"),
            P("dp", None, "tp"),
        ),
        check_vma=False,
    )
```

time: 80.7 us -> 75.9 us (0.941)
  blocking collectives: 51.1 us -> 47.5 us
  starting transfers between devices: 10.8 us -> 9.5 us
    all_to_all x3, blocking collectives: 51.1 us -> 47.5 us  [exchange(): return lax.all_to_all(array, 'kv', split_axis=0, concat_axis=0, tiled=True)]
    all_to_all x1, starting transfers between devices: 5.66 us -> 3.87 us  [exchange(): return lax.all_to_all(array, 'kv', split_axis=0, concat_axis=0, tiled=True)]
where the time goes in v3:
time: 75.9 us; the launch traced here: 75.5 us
  blocking collectives  47.5 us (63%)
  Pallas kernels  10.3 us (14%)
  starting transfers between devices  9.5 us (13%)
  waiting for transfers between devices  6.2 us (8%)
    all_to_all x3, blocking collectives, exchange(): return lax.all_to_all(array, 'kv', split_axis=0, concat_axis=0, tiled=True)  47.5 us
    all_to_all x1, waiting for transfers between devices, exchange(): return lax.all_to_all(array, 'kv', split_axis=0, concat_axis=0, tiled=True)  6.19 us
    ppermute x1, starting transfers between devices, shards(): other = lax.ppermute(term, 'tp', [(0, 1), (1, 0)])  5.63 us
    all_to_all x1, starting transfers between devices, exchange(): return lax.all_to_all(array, 'kv', split_axis=0, concat_axis=0, tiled=True)  3.87 us
    pallas_call x1, Pallas kernels, shards(): pl.pallas_call(stage_kernel, out_shape=(cache, jax.ShapeDtypeStruct((HELD...  3.69 us
    pallas_call x1, Pallas kernels, shards(): pl.pallas_call(attend_kernel, out_shape=(jax.ShapeDtypeStruct((N_KV * SEN...  2.81 us
  transfers between devices with their start and end apart: 2, of which 1 were waited for; matrix products, arithmetic and copies ran while one was open for 0% of the time, Pallas kernels for 6%

profile of v3, /device:TPU:1, one launch (start us, length us, event | category | flops | bytes accessed | tf_op | source)
XLA Modules:
  0.0 75.5 jit_solution(14828215232258122083)
XLA Ops:
  0.6 1.3 %project.1 = (f32[288,128]{1,0:T(8,128)S(1)}, bf16[32,24,128]{2,1,0:T(8,128)(2,1)S(1)}, f32[8,128]{1,0:T(8,128)S(1)}) custom-call(bf16[4,16,64]{2,1,0:T(8,128)(2,1)} %x_hbm.1, f32[1,64]{1,0:T(1,128)} %bitcast.23, bf16[64,512]{1,0:T(8,128)(2,1)} %wq_hbm.1, bf16[64,512]{1,0:T(8,128)(2,1)} %wk_hbm.1, bf16[64,512]{1,0:T(8,128)(2,1)} %wv_hbm.1, ...), custom_call_target="tpu_custom_call" | custom-call | flops 13000000 | bytes 700000 | tf_op jit(solution)/shard_map/project/pallas_call | solution.py:478
  2.0 21.1 %all_to_all.20 = f32[32,1,1152]{2,1,0:T(1,128)S(1)} all-to-all(f32[32,1,1152]{2,1,0:T(1,128)S(1)} %bitcast.19), channel_id=1, replica_groups=mesh['dp'=4,'kv'=32,'tp'=2] {'kv'}, dimensions={0} | all-to-all | bytes 294912 | tf_op jit(solution)/shard_map/all_to_all | solution.py:449
  23.1 1.0 %finish.1 = (bf16[32,32,128]{2,1,0:T(8,128)(2,1)}, f32[1,128]{1,0:T(1,128)S(1)}, f32[8,128]{1,0:T(8,128)S(1)}) custom-call(f32[288,128]{1,0:T(8,128)S(1)} %bitcast.17, bf16[32,24,128]{2,1,0:T(8,128)(2,1)S(1)} %get-tuple-element.34.part_ref, f32[8,128]{1,0:T(8,128)S(1)} %get-tuple-element.32.consts_ref), custom_call_target="tpu_custom_call" | custom-call | flops 1000000 | bytes 700000 | tf_op jit(solution)/shard_map/finish/pallas_call | solution.py:516
  24.1 3.9 %all-to-all-start.1 = ((bf16[32,32,128]{2,1,0:T(8,128)(2,1)}), bf16[32,32,128]{2,1,0:T(8,128)(2,1)S(1)}, u32[]{:S(2)}, u32[]{:S(2)}) async-start(bf16[32,32,128]{2,1,0:T(8,128)(2,1)} %get-tuple-element.42), calls=%async_computation.1 | async-start | bytes 524288 | tf_op jit(solution)/shard_map/all_to_all | solution.py:449
  28.0 0.0 copy-start.1
  28.0 0.7 copy-done.1
  28.7 3.7 %stage.1 = (bf16[4,512,512]{2,1,0:T(8,128)(2,1)S(1)}, bf16[2,512,512]{2,1,0:T(8,128)(2,1)S(1)}, f32[4,8,512]{2,1,0:T(8,128)S(1)}, f32[16,16]{1,0:T(8,128)S(1)}, ...) custom-call(bf16[4,512,512]{2,1,0:T(8,128)(2,1)} %key_hbm.1, bf16[4,512,512]{2,1,0:T(8,128)(2,1)} %value_hbm.2, ...), custom_call_target="tpu_custom_call" | custom-call | flops 500000000 | bytes 8500000 | tf_op jit(solution)/shard_map/stage/pallas_call | solution.py:533
  32.4 6.2 %all-to-all-done.1.got_ref = bf16[32,32,128]{2,1,0:T(8,128)(2,1)S(1)} async-done(((bf16[32,32,128]{2,1,0:T(8,128)(2,1)}), bf16[32,32,128]{2,1,0:T(8,128)(2,1)S(1)}, u32[]{:S(2)}, u32[]{:S(2)}) %all-to-all-start.1) | async-done | bytes 262176 | tf_op jit(solution)/shard_map/all_to_all | solution.py:449
  38.6 0.0 copy-start
  38.6 2.8 %attend.1 = (f32[288,128]{1,0:T(8,128)S(1)}, f32[16,128]{1,0:T(8,128)S(1)}, bf16[16,128]{1,0:T(8,128)(2,1)S(1)}) custom-call(f32[8,128]{1,0:T(8,128)S(1)} %get-tuple-element.32.consts_ref, f32[8,128]{1,0:T(8,128)S(1)} %get-tuple-element.35.inverse_ref, f32[1,128]{1,0:T(1,128)S(1)} %get-tuple-element.37.row_ref, f32[16,16]{1,0:T(8,128)S(1)} %get-tuple-element.41.bias_ref, ...), custom_call_target="tpu_custom_call" | custom-call | flops 600000000 | bytes 4500000 | tf_op jit(solution)/shard_map/attend/pallas_call | solution.py:554
  41.4 13.3 %all_to_all.21 = f32[32,1,1152]{2,1,0:T(1,128)S(1)} all-to-all(f32[32,1,1152]{2,1,0:T(1,128)S(1)} %bitcast.18), channel_id=1, replica_groups=mesh['dp'=4,'kv'=32,'tp'=2] {'kv'}, dimensions={0} | all-to-all | bytes 294912 | tf_op jit(solution)/shard_map/all_to_all | solution.py:449
  54.7 0.4 merge.1
  55.1 13.0 %all_to_all.22.got_ref = bf16[32,24,128]{2,1,0:T(8,128)(2,1)S(1)} all-to-all(bf16[32,24,128]{2,1,0:T(8,128)(2,1)S(1)} %merge.1), channel_id=1, replica_groups=mesh['dp'=4,'kv'=32,'tp'=2] {'kv'}, dimensions={0} | all-to-all | bytes 393216 | tf_op jit(solution)/shard_map/all_to_all | solution.py:449
  68.1 0.0 copy-done
  68.1 0.2 out.1
  68.3 5.6 %collective-permute-start = (bf16[64,64]{1,0:T(8,128)(2,1)S(1)}, bf16[64,64]{1,0:T(8,128)(2,1)S(1)}, u32[]{:S(2)}, u32[]{:S(2)}) collective-permute-start(bf16[64,64]{1,0:T(8,128)(2,1)S(1)} %out.1), channel_id=1, source_target_pairs={{0,1},{1,0},{2,3},{3,2},{4,5},{5,4},{6,7},{7,6},{8,9},{9,8},{10,11... | collective-permute-start | bytes 24584 | tf_op jit(solution)/shard_map/ppermute | solution.py:592
  73.9 0.9 %write.1 = (bf16[4,512,512]{2,1,0:T(8,128)(2,1)}, bf16[4,512,512]{2,1,0:T(8,128)(2,1)}, f32[4,8,16]{2,1,0:T(8,128)}) custom-call(f32[8,128]{1,0:T(8,128)S(1)} %get-tuple-element.32.consts_ref, f32[288,128]{1,0:T(8,128)S(1)} %bitcast.16, bf16[32,24,128]{2,1,0:T(8,128)(2,1)S(1)} %all_to_all.22.got_ref, ...), custom_call_target="tpu_custom_call", output_to_operand_aliasing={{0}: (5, {}), {1}: (6, {})} | custom-call | flops 60000000 | bytes 1000000 | tf_op jit(solution)/shard_map/write/pallas_call | solution.py:594
  74.9 0.0 collective-permute-done
  74.9 0.6 add_convert_fusion
Async XLA Ops:
  24.1 14.4 %all-to-all-start.1 = ((bf16[32,32,128]{2,1,0:T(8,128)(2,1)}), bf16[32,32,128]{2,1,0:T(8,128)(2,1)S(1)}, u32[]{:S(2)}, u32[]{:S(2)}) async-start(bf16[32,32,128]{2,1,0:T(8,128)(2,1)} %get-tuple-element.42), calls=%async_computation.1 | async-start | bytes 524288 | tf_op jit(solution)/shard_map/all_to_all | solution.py:449
  28.0 0.7 copy-start.1
  38.6 29.5 %copy-start = (bf16[512,64]{0,1:T(8,128)(2,1)S(1)}, bf16[512,64]{0,1:T(8,128)(2,1)}, u32[]{:S(2)}) copy-start(bf16[512,64]{0,1:T(8,128)(2,1)} %param.27) | copy-start | bytes 196612
  68.3 6.6 %collective-permute-start = (bf16[64,64]{1,0:T(8,128)(2,1)S(1)}, bf16[64,64]{1,0:T(8,128)(2,1)S(1)}, u32[]{:S(2)}, u32[]{:S(2)}) collective-permute-start(bf16[64,64]{1,0:T(8,128)(2,1)S(1)} %out.1), channel_id=1, source_target_pairs={{0,1},{1,0},{2,3},{3,2},{4,5},{5,4},{6,7},{7,6},{8,9},{9,8},{10,11... | collective-permute-start | bytes 24584 | tf_op jit(solution)/shard_map/ppermute | solution.py:592

commit v4 on v3

--- a/solution.py
+++ b/solution.py
@@ -243,10 +243,15 @@
     consts_ref, inverse_ref, row_ref, bias_ref, got_ref, key_ref, held_ref, gate_ref, value_hbm,
     out_ref, tree_ref, own_ref, rest_ref, weights_ref, sems,
 ):
-    loads = {}
-    for s in range(HELD, SEQS):
-        loads[s] = pltpu.make_async_copy(value_hbm.at[s], rest_ref.at[s - HELD], sems.at[s])
-        loads[s].start()
+    loads = {
+        s: pltpu.make_async_copy(value_hbm.at[s], rest_ref.at[s - HELD], sems.at[s])
+        for s in range(HELD, SEQS)
+    }
+
+    @pl.loop(HELD, SEQS)
+    def _(s):
+        pltpu.make_async_copy(value_hbm.at[s], rest_ref.at[s - HELD], sems.at[s]).start()
+
     sums = []
     for s in range(SEQS):
         raw = score_sequence(s, got_ref, key_ref)

time: 75.9 us -> 75.3 us (level)
  no operation moved by 1% of the time
where the time goes in v4:
time: 75.3 us; the launch traced here: 74.9 us
  blocking collectives  47.5 us (63%)
  Pallas kernels  9.72 us (13%)
  starting transfers between devices  9.54 us (13%)
  waiting for transfers between devices  6.2 us (8%)
    all_to_all x3, blocking collectives, exchange(): return lax.all_to_all(array, 'kv', split_axis=0, concat_axis=0, tiled=True)  47.5 us
    all_to_all x1, waiting for transfers between devices, exchange(): return lax.all_to_all(array, 'kv', split_axis=0, concat_axis=0, tiled=True)  6.19 us
    ppermute x1, starting transfers between devices, shards(): other = lax.ppermute(term, 'tp', [(0, 1), (1, 0)])  5.68 us
    all_to_all x1, starting transfers between devices, exchange(): return lax.all_to_all(array, 'kv', split_axis=0, concat_axis=0, tiled=True)  3.87 us
    pallas_call x1, Pallas kernels, shards(): pl.pallas_call(stage_kernel, out_shape=(cache, jax.ShapeDtypeStruct((HELD...  3.69 us
    pallas_call x1, Pallas kernels, shards(): pl.pallas_call(attend_kernel, out_shape=(jax.ShapeDtypeStruct((N_KV * SEN...  2.2 us
  transfers between devices with their start and end apart: 2, of which 1 were waited for; matrix products, arithmetic and copies ran while one was open for 0% of the time, Pallas kernels for 6%

profile of v4, /device:TPU:1, one launch (start us, length us, event | category | flops | bytes accessed | tf_op | source)
XLA Modules:
  0.0 74.9 jit_solution(8503813804813534840)
XLA Ops:
  0.6 1.3 %project.1 = (f32[288,128]{1,0:T(8,128)S(1)}, bf16[32,24,128]{2,1,0:T(8,128)(2,1)S(1)}, f32[8,128]{1,0:T(8,128)S(1)}) custom-call(bf16[4,16,64]{2,1,0:T(8,128)(2,1)} %x_hbm.1, f32[1,64]{1,0:T(1,128)} %bitcast.23, bf16[64,512]{1,0:T(8,128)(2,1)} %wq_hbm.1, bf16[64,512]{1,0:T(8,128)(2,1)} %wk_hbm.1, bf16[64,512]{1,0:T(8,128)(2,1)} %wv_hbm.1, ...), custom_call_target="tpu_custom_call" | custom-call | flops 13000000 | bytes 700000 | tf_op jit(solution)/shard_map/project/pallas_call | solution.py:483
  2.0 21.1 %all_to_all.20 = f32[32,1,1152]{2,1,0:T(1,128)S(1)} all-to-all(f32[32,1,1152]{2,1,0:T(1,128)S(1)} %bitcast.19), channel_id=1, replica_groups=mesh['dp'=4,'kv'=32,'tp'=2] {'kv'}, dimensions={0} | all-to-all | bytes 294912 | tf_op jit(solution)/shard_map/all_to_all | solution.py:454
  23.1 1.0 %finish.1 = (bf16[32,32,128]{2,1,0:T(8,128)(2,1)}, f32[1,128]{1,0:T(1,128)S(1)}, f32[8,128]{1,0:T(8,128)S(1)}) custom-call(f32[288,128]{1,0:T(8,128)S(1)} %bitcast.17, bf16[32,24,128]{2,1,0:T(8,128)(2,1)S(1)} %get-tuple-element.34.part_ref, f32[8,128]{1,0:T(8,128)S(1)} %get-tuple-element.32.consts_ref), custom_call_target="tpu_custom_call" | custom-call | flops 1000000 | bytes 700000 | tf_op jit(solution)/shard_map/finish/pallas_call | solution.py:521
  24.1 3.9 %all-to-all-start.1 = ((bf16[32,32,128]{2,1,0:T(8,128)(2,1)}), bf16[32,32,128]{2,1,0:T(8,128)(2,1)S(1)}, u32[]{:S(2)}, u32[]{:S(2)}) async-start(bf16[32,32,128]{2,1,0:T(8,128)(2,1)} %get-tuple-element.42), calls=%async_computation.1 | async-start | bytes 524288 | tf_op jit(solution)/shard_map/all_to_all | solution.py:454
  28.0 0.0 copy-start.1
  28.0 0.7 copy-done.1
  28.7 3.7 %stage.1 = (bf16[4,512,512]{2,1,0:T(8,128)(2,1)S(1)}, bf16[2,512,512]{2,1,0:T(8,128)(2,1)S(1)}, f32[4,8,512]{2,1,0:T(8,128)S(1)}, f32[16,16]{1,0:T(8,128)S(1)}, ...) custom-call(bf16[4,512,512]{2,1,0:T(8,128)(2,1)} %key_hbm.1, bf16[4,512,512]{2,1,0:T(8,128)(2,1)} %value_hbm.2, ...), custom_call_target="tpu_custom_call" | custom-call | flops 500000000 | bytes 8500000 | tf_op jit(solution)/shard_map/stage/pallas_call | solution.py:538
  32.4 6.2 %all-to-all-done.1.got_ref = bf16[32,32,128]{2,1,0:T(8,128)(2,1)S(1)} async-done(((bf16[32,32,128]{2,1,0:T(8,128)(2,1)}), bf16[32,32,128]{2,1,0:T(8,128)(2,1)S(1)}, u32[]{:S(2)}, u32[]{:S(2)}) %all-to-all-start.1) | async-done | bytes 262176 | tf_op jit(solution)/shard_map/all_to_all | solution.py:454
  38.6 0.0 copy-start
  38.6 2.2 %attend.1 = (f32[288,128]{1,0:T(8,128)S(1)}, f32[16,128]{1,0:T(8,128)S(1)}, bf16[16,128]{1,0:T(8,128)(2,1)S(1)}) custom-call(f32[8,128]{1,0:T(8,128)S(1)} %get-tuple-element.32.consts_ref, f32[8,128]{1,0:T(8,128)S(1)} %get-tuple-element.35.inverse_ref, f32[1,128]{1,0:T(1,128)S(1)} %get-tuple-element.37.row_ref, f32[16,16]{1,0:T(8,128)S(1)} %get-tuple-element.41.bias_ref, ...), custom_call_target="tpu_custom_call" | custom-call | flops 600000000 | bytes 4500000 | tf_op jit(solution)/shard_map/attend/pallas_call | solution.py:559
  40.8 13.3 %all_to_all.21 = f32[32,1,1152]{2,1,0:T(1,128)S(1)} all-to-all(f32[32,1,1152]{2,1,0:T(1,128)S(1)} %bitcast.18), channel_id=1, replica_groups=mesh['dp'=4,'kv'=32,'tp'=2] {'kv'}, dimensions={0} | all-to-all | bytes 294912 | tf_op jit(solution)/shard_map/all_to_all | solution.py:454
  54.1 0.4 merge.1
  54.5 13.0 %all_to_all.22.got_ref = bf16[32,24,128]{2,1,0:T(8,128)(2,1)S(1)} all-to-all(bf16[32,24,128]{2,1,0:T(8,128)(2,1)S(1)} %merge.1), channel_id=1, replica_groups=mesh['dp'=4,'kv'=32,'tp'=2] {'kv'}, dimensions={0} | all-to-all | bytes 393216 | tf_op jit(solution)/shard_map/all_to_all | solution.py:454
  67.5 0.0 copy-done
  67.5 0.2 out.1
  67.7 5.7 %collective-permute-start = (bf16[64,64]{1,0:T(8,128)(2,1)S(1)}, bf16[64,64]{1,0:T(8,128)(2,1)S(1)}, u32[]{:S(2)}, u32[]{:S(2)}) collective-permute-start(bf16[64,64]{1,0:T(8,128)(2,1)S(1)} %out.1), channel_id=1, source_target_pairs={{0,1},{1,0},{2,3},{3,2},{4,5},{5,4},{6,7},{7,6},{8,9},{9,8},{10,11... | collective-permute-start | bytes 24584 | tf_op jit(solution)/shard_map/ppermute | solution.py:597
  73.3 0.9 %write.1 = (bf16[4,512,512]{2,1,0:T(8,128)(2,1)}, bf16[4,512,512]{2,1,0:T(8,128)(2,1)}, f32[4,8,16]{2,1,0:T(8,128)}) custom-call(f32[8,128]{1,0:T(8,128)S(1)} %get-tuple-element.32.consts_ref, f32[288,128]{1,0:T(8,128)S(1)} %bitcast.16, bf16[32,24,128]{2,1,0:T(8,128)(2,1)S(1)} %all_to_all.22.got_ref, ...), custom_call_target="tpu_custom_call", output_to_operand_aliasing={{0}: (5, {}), {1}: (6, {})} | custom-call | flops 60000000 | bytes 1000000 | tf_op jit(solution)/shard_map/write/pallas_call | solution.py:599
  74.3 0.0 collective-permute-done
  74.3 0.6 add_convert_fusion
Async XLA Ops:
  24.1 14.4 %all-to-all-start.1 = ((bf16[32,32,128]{2,1,0:T(8,128)(2,1)}), bf16[32,32,128]{2,1,0:T(8,128)(2,1)S(1)}, u32[]{:S(2)}, u32[]{:S(2)}) async-start(bf16[32,32,128]{2,1,0:T(8,128)(2,1)} %get-tuple-element.42), calls=%async_computation.1 | async-start | bytes 524288 | tf_op jit(solution)/shard_map/all_to_all | solution.py:454
  28.0 0.7 copy-start.1
  38.6 28.9 %copy-start = (bf16[512,64]{0,1:T(8,128)(2,1)S(1)}, bf16[512,64]{0,1:T(8,128)(2,1)}, u32[]{:S(2)}) copy-start(bf16[512,64]{0,1:T(8,128)(2,1)} %param.27) | copy-start | bytes 196612
  67.7 6.6 %collective-permute-start = (bf16[64,64]{1,0:T(8,128)(2,1)S(1)}, bf16[64,64]{1,0:T(8,128)(2,1)S(1)}, u32[]{:S(2)}, u32[]{:S(2)}) collective-permute-start(bf16[64,64]{1,0:T(8,128)(2,1)S(1)} %out.1), channel_id=1, source_target_pairs={{0,1},{1,0},{2,3},{3,2},{4,5},{5,4},{6,7},{7,6},{8,9},{9,8},{10,11... | collective-permute-start | bytes 24584 | tf_op jit(solution)/shard_map/ppermute | solution.py:597

commit v5 on v4

--- a/solution.py
+++ b/solution.py
@@ -22,11 +22,11 @@
 SEQS = 4
 BLOCK = 512
 SEND_A = 9
-SEND_KV = 24
+SEND_KV = 32
 SEND_B = SUB + SEND_KV
 SEND_C = 9
 SEND_D = 24
-HELD = 2
+HELD = 1
 
 
 def iota(shape, dim):
@@ -153,8 +153,10 @@
                 out_ref[SEND_A * peer + SUB : SEND_A * (peer + 1), :] = jnp.concatenate(
                     [own[head : head + 1], square_row], axis=1
                 )
-                high = key[j].astype(BF16).astype(F32)
-                part_ref[peer] = jnp.concatenate([high, key[j] - high, value[j]], axis=0).astype(BF16)
+                highs = [x.astype(BF16).astype(F32) for x in (key[j], value[j])]
+                part_ref[peer] = jnp.concatenate(
+                    [highs[0], key[j] - highs[0], highs[1], value[j] - highs[1]], axis=0
+                ).astype(BF16)
 
 
 def head_scale(block):
@@ -321,9 +323,9 @@
     key = jnp.zeros((SUB, LANES), F32)
     value = jnp.zeros((SUB, LANES), F32)
     for p in range(N_KV):
-        high, low, part = (got_ref[p, SUB * i : SUB * i + SUB].astype(F32) for i in range(1, 4))
-        key = key + (high + low)
-        value = value + part
+        part = [got_ref[p, SUB * i : SUB * i + SUB].astype(F32) for i in range(1, 5)]
+        key = key + (part[0] + part[1])
+        value = value + (part[2] + part[3])
     inverse = inverse_ref[...]
     key = key * inverse
     key = (key * head_scale(key) * consts_ref[1:2]).astype(BF16).astype(F32)

time: 75.3 us -> 77 us (1.023)
  blocking collectives: 47.5 us -> 49.3 us
  starting transfers between devices: 9.54 us -> 8.5 us
    all_to_all x3, blocking collectives: 47.5 us -> 49.3 us  [exchange(): return lax.all_to_all(array, 'kv', split_axis=0, concat_axis=0, tiled=True)]
    ppermute x1, starting transfers between devices: 5.68 us -> 4.62 us  [shards(): other = lax.ppermute(term, 'tp', [(0, 1), (1, 0)])]
where the time goes in v5:
time: 77 us; the launch traced here: 76.5 us
  blocking collectives  49.3 us (64%)
  Pallas kernels  10.1 us (13%)
  starting transfers between devices  8.5 us (11%)
  waiting for transfers between devices  6.67 us (9%)
    all_to_all x3, blocking collectives, exchange(): return lax.all_to_all(array, 'kv', split_axis=0, concat_axis=0, tiled=True)  49.3 us
    all_to_all x1, waiting for transfers between devices, exchange(): return lax.all_to_all(array, 'kv', split_axis=0, concat_axis=0, tiled=True)  6.67 us
    ppermute x1, starting transfers between devices, shards(): other = lax.ppermute(term, 'tp', [(0, 1), (1, 0)])  4.62 us
    all_to_all x1, starting transfers between devices, exchange(): return lax.all_to_all(array, 'kv', split_axis=0, concat_axis=0, tiled=True)  3.87 us
    pallas_call x1, Pallas kernels, shards(): pl.pallas_call(stage_kernel, out_shape=(cache, jax.ShapeDtypeStruct((HELD...  3.69 us
    pallas_call x1, Pallas kernels, shards(): pl.pallas_call(attend_kernel, out_shape=(jax.ShapeDtypeStruct((N_KV * SEN...  2.5 us
  transfers between devices with their start and end apart: 2, of which 1 were waited for; matrix products, arithmetic and copies ran while one was open for 0% of the time, Pallas kernels for 6%

profile of v5, /device:TPU:1, one launch (start us, length us, event | category | flops | bytes accessed | tf_op | source)
XLA Modules:
  0.0 76.5 jit_solution(15589765782940530774)
XLA Ops:
  0.6 1.4 %project.1 = (f32[288,128]{1,0:T(8,128)S(1)}, bf16[32,32,128]{2,1,0:T(8,128)(2,1)S(1)}, f32[8,128]{1,0:T(8,128)S(1)}) custom-call(bf16[4,16,64]{2,1,0:T(8,128)(2,1)} %x_hbm.1, f32[1,64]{1,0:T(1,128)} %bitcast.23, bf16[64,512]{1,0:T(8,128)(2,1)} %wq_hbm.1, bf16[64,512]{1,0:T(8,128)(2,1)} %wk_hbm.1, bf16[64,512]{1,0:T(8,128)(2,1)} %wv_hbm.1, ...), custom_call_target="tpu_custom_call" | custom-call | flops 13000000 | bytes 700000 | tf_op jit(solution)/shard_map/project/pallas_call | solution.py:485
  2.0 21.1 %all_to_all.20 = f32[32,1,1152]{2,1,0:T(1,128)S(1)} all-to-all(f32[32,1,1152]{2,1,0:T(1,128)S(1)} %bitcast.19), channel_id=1, replica_groups=mesh['dp'=4,'kv'=32,'tp'=2] {'kv'}, dimensions={0} | all-to-all | bytes 294912 | tf_op jit(solution)/shard_map/all_to_all | solution.py:456
  23.1 1.0 %finish.1 = (bf16[32,40,128]{2,1,0:T(8,128)(2,1)}, f32[1,128]{1,0:T(1,128)S(1)}, f32[8,128]{1,0:T(8,128)S(1)}) custom-call(f32[288,128]{1,0:T(8,128)S(1)} %bitcast.17, bf16[32,32,128]{2,1,0:T(8,128)(2,1)S(1)} %get-tuple-element.34.part_ref, f32[8,128]{1,0:T(8,128)S(1)} %get-tuple-element.32.consts_ref), custom_call_target="tpu_custom_call" | custom-call | flops 1000000 | bytes 700000 | tf_op jit(solution)/shard_map/finish/pallas_call | solution.py:523
  24.1 3.9 %all-to-all-start.1 = ((bf16[32,40,128]{2,1,0:T(8,128)(2,1)}), bf16[32,40,128]{2,1,0:T(8,128)(2,1)S(1)}, u32[]{:S(2)}, u32[]{:S(2)}) async-start(bf16[32,40,128]{2,1,0:T(8,128)(2,1)} %get-tuple-element.42), calls=%async_computation.1 | async-start | bytes 655360 | tf_op jit(solution)/shard_map/all_to_all | solution.py:456
  28.0 0.0 copy-start.1
  28.0 0.7 copy-done.1
  28.7 3.7 %stage.1 = (bf16[4,512,512]{2,1,0:T(8,128)(2,1)S(1)}, bf16[1,512,512]{2,1,0:T(8,128)(2,1)S(1)}, f32[4,8,512]{2,1,0:T(8,128)S(1)}, f32[16,16]{1,0:T(8,128)S(1)}, ...) custom-call(bf16[4,512,512]{2,1,0:T(8,128)(2,1)} %key_hbm.1, bf16[4,512,512]{2,1,0:T(8,128)(2,1)} %value_hbm.2, ...), custom_call_target="tpu_custom_call" | custom-call | flops 500000000 | bytes 8500000 | tf_op jit(solution)/shard_map/stage/pallas_call | solution.py:540
  32.4 6.7 %all-to-all-done.1.got_ref = bf16[32,40,128]{2,1,0:T(8,128)(2,1)S(1)} async-done(((bf16[32,40,128]{2,1,0:T(8,128)(2,1)}), bf16[32,40,128]{2,1,0:T(8,128)(2,1)S(1)}, u32[]{:S(2)}, u32[]{:S(2)}) %all-to-all-start.1) | async-done | bytes 327712 | tf_op jit(solution)/shard_map/all_to_all | solution.py:456
  39.1 0.0 copy-start
  39.1 2.5 %attend.1 = (f32[288,128]{1,0:T(8,128)S(1)}, f32[16,128]{1,0:T(8,128)S(1)}, bf16[16,128]{1,0:T(8,128)(2,1)S(1)}) custom-call(f32[8,128]{1,0:T(8,128)S(1)} %get-tuple-element.32.consts_ref, f32[8,128]{1,0:T(8,128)S(1)} %get-tuple-element.35.inverse_ref, f32[1,128]{1,0:T(1,128)S(1)} %get-tuple-element.37.row_ref, f32[16,16]{1,0:T(8,128)S(1)} %get-tuple-element.41.bias_ref, ...), custom_call_target="tpu_custom_call" | custom-call | flops 600000000 | bytes 4500000 | tf_op jit(solution)/shard_map/attend/pallas_call | solution.py:561
  41.6 14.9 %all_to_all.21 = f32[32,1,1152]{2,1,0:T(1,128)S(1)} all-to-all(f32[32,1,1152]{2,1,0:T(1,128)S(1)} %bitcast.18), channel_id=1, replica_groups=mesh['dp'=4,'kv'=32,'tp'=2] {'kv'}, dimensions={0} | all-to-all | bytes 294912 | tf_op jit(solution)/shard_map/all_to_all | solution.py:456
  56.5 0.4 merge.1
  56.8 13.3 %all_to_all.22.got_ref = bf16[32,24,128]{2,1,0:T(8,128)(2,1)S(1)} all-to-all(bf16[32,24,128]{2,1,0:T(8,128)(2,1)S(1)} %merge.1), channel_id=1, replica_groups=mesh['dp'=4,'kv'=32,'tp'=2] {'kv'}, dimensions={0} | all-to-all | bytes 393216 | tf_op jit(solution)/shard_map/all_to_all | solution.py:456
  70.1 0.0 copy-done
  70.1 0.2 out.1
  70.4 4.6 %collective-permute-start = (bf16[64,64]{1,0:T(8,128)(2,1)S(1)}, bf16[64,64]{1,0:T(8,128)(2,1)S(1)}, u32[]{:S(2)}, u32[]{:S(2)}) collective-permute-start(bf16[64,64]{1,0:T(8,128)(2,1)S(1)} %out.1), channel_id=1, source_target_pairs={{0,1},{1,0},{2,3},{3,2},{4,5},{5,4},{6,7},{7,6},{8,9},{9,8},{10,11... | collective-permute-start | bytes 24584 | tf_op jit(solution)/shard_map/ppermute | solution.py:599
  75.0 0.9 %write.1 = (bf16[4,512,512]{2,1,0:T(8,128)(2,1)}, bf16[4,512,512]{2,1,0:T(8,128)(2,1)}, f32[4,8,16]{2,1,0:T(8,128)}) custom-call(f32[8,128]{1,0:T(8,128)S(1)} %get-tuple-element.32.consts_ref, f32[288,128]{1,0:T(8,128)S(1)} %bitcast.16, bf16[32,24,128]{2,1,0:T(8,128)(2,1)S(1)} %all_to_all.22.got_ref, ...), custom_call_target="tpu_custom_call", output_to_operand_aliasing={{0}: (5, {}), {1}: (6, {})} | custom-call | flops 60000000 | bytes 1000000 | tf_op jit(solution)/shard_map/write/pallas_call | solution.py:601
  75.9 0.0 collective-permute-done
  75.9 0.6 add_convert_fusion
Async XLA Ops:
  24.1 14.9 %all-to-all-start.1 = ((bf16[32,40,128]{2,1,0:T(8,128)(2,1)}), bf16[32,40,128]{2,1,0:T(8,128)(2,1)S(1)}, u32[]{:S(2)}, u32[]{:S(2)}) async-start(bf16[32,40,128]{2,1,0:T(8,128)(2,1)} %get-tuple-element.42), calls=%async_computation.1 | async-start | bytes 655360 | tf_op jit(solution)/shard_map/all_to_all | solution.py:456
  28.0 0.7 copy-start.1
  39.1 31.1 %copy-start = (bf16[512,64]{0,1:T(8,128)(2,1)S(1)}, bf16[512,64]{0,1:T(8,128)(2,1)}, u32[]{:S(2)}) copy-start(bf16[512,64]{0,1:T(8,128)(2,1)} %param.27) | copy-start | bytes 196612
  70.4 5.6 %collective-permute-start = (bf16[64,64]{1,0:T(8,128)(2,1)S(1)}, bf16[64,64]{1,0:T(8,128)(2,1)S(1)}, u32[]{:S(2)}, u32[]{:S(2)}) collective-permute-start(bf16[64,64]{1,0:T(8,128)(2,1)S(1)} %out.1), channel_id=1, source_target_pairs={{0,1},{1,0},{2,3},{3,2},{4,5},{5,4},{6,7},{7,6},{8,9},{9,8},{10,11... | collective-permute-start | bytes 24584 | tf_op jit(solution)/shard_map/ppermute | solution.py:599

commit v6 on v4

--- a/solution.py
+++ b/solution.py
@@ -259,8 +259,9 @@
     attend_tree(consts_ref, inverse_ref, bias_ref, got_ref, tree_ref, own_ref)
     tail = row_ref[...]
     for s in range(SEQS):
-        if s in loads:
-            loads[s].wait()
+        if s == HELD:
+            for load in loads.values():
+                load.wait()
         values = held_ref[s] if s < HELD else rest_ref[s - HELD]
         send_sequence(s, dot_nn(weights_ref[s], values), *sums[s], tail, out_ref)
 

time: 75.3 us -> 75.1 us (level)
  no operation moved by 1% of the time
where the time goes in v6:
time: 75.1 us; the launch traced here: 74.7 us
  blocking collectives  47.5 us (63%)
  starting transfers between devices  9.54 us (13%)
  Pallas kernels  9.48 us (13%)
  waiting for transfers between devices  6.2 us (8%)
    all_to_all x3, blocking collectives, exchange(): return lax.all_to_all(array, 'kv', split_axis=0, concat_axis=0, tiled=True)  47.5 us
    all_to_all x1, waiting for transfers between devices, exchange(): return lax.all_to_all(array, 'kv', split_axis=0, concat_axis=0, tiled=True)  6.19 us
    ppermute x1, starting transfers between devices, shards(): other = lax.ppermute(term, 'tp', [(0, 1), (1, 0)])  5.67 us
    all_to_all x1, starting transfers between devices, exchange(): return lax.all_to_all(array, 'kv', split_axis=0, concat_axis=0, tiled=True)  3.87 us
    pallas_call x1, Pallas kernels, shards(): pl.pallas_call(stage_kernel, out_shape=(cache, jax.ShapeDtypeStruct((HELD...  3.69 us
    pallas_call x1, Pallas kernels, shards(): pl.pallas_call(attend_kernel, out_shape=(jax.ShapeDtypeStruct((N_KV * SEN...  1.97 us
  transfers between devices with their start and end apart: 2, of which 1 were waited for; matrix products, arithmetic and copies ran while one was open for 0% of the time, Pallas kernels for 6%

profile of v6, /device:TPU:1, one launch (start us, length us, event | category | flops | bytes accessed | tf_op | source)
XLA Modules:
  0.0 74.7 jit_solution(9593997820170584092)
XLA Ops:
  0.6 1.3 %project.1 = (f32[288,128]{1,0:T(8,128)S(1)}, bf16[32,24,128]{2,1,0:T(8,128)(2,1)S(1)}, f32[8,128]{1,0:T(8,128)S(1)}) custom-call(bf16[4,16,64]{2,1,0:T(8,128)(2,1)} %x_hbm.1, f32[1,64]{1,0:T(1,128)} %bitcast.23, bf16[64,512]{1,0:T(8,128)(2,1)} %wq_hbm.1, bf16[64,512]{1,0:T(8,128)(2,1)} %wk_hbm.1, bf16[64,512]{1,0:T(8,128)(2,1)} %wv_hbm.1, ...), custom_call_target="tpu_custom_call" | custom-call | flops 13000000 | bytes 700000 | tf_op jit(solution)/shard_map/project/pallas_call | solution.py:484
  2.0 21.1 %all_to_all.20 = f32[32,1,1152]{2,1,0:T(1,128)S(1)} all-to-all(f32[32,1,1152]{2,1,0:T(1,128)S(1)} %bitcast.19), channel_id=1, replica_groups=mesh['dp'=4,'kv'=32,'tp'=2] {'kv'}, dimensions={0} | all-to-all | bytes 294912 | tf_op jit(solution)/shard_map/all_to_all | solution.py:455
  23.1 1.0 %finish.1 = (bf16[32,32,128]{2,1,0:T(8,128)(2,1)}, f32[1,128]{1,0:T(1,128)S(1)}, f32[8,128]{1,0:T(8,128)S(1)}) custom-call(f32[288,128]{1,0:T(8,128)S(1)} %bitcast.17, bf16[32,24,128]{2,1,0:T(8,128)(2,1)S(1)} %get-tuple-element.34.part_ref, f32[8,128]{1,0:T(8,128)S(1)} %get-tuple-element.32.consts_ref), custom_call_target="tpu_custom_call" | custom-call | flops 1000000 | bytes 700000 | tf_op jit(solution)/shard_map/finish/pallas_call | solution.py:522
  24.1 3.9 %all-to-all-start.1 = ((bf16[32,32,128]{2,1,0:T(8,128)(2,1)}), bf16[32,32,128]{2,1,0:T(8,128)(2,1)S(1)}, u32[]{:S(2)}, u32[]{:S(2)}) async-start(bf16[32,32,128]{2,1,0:T(8,128)(2,1)} %get-tuple-element.42), calls=%async_computation.1 | async-start | bytes 524288 | tf_op jit(solution)/shard_map/all_to_all | solution.py:455
  28.0 0.0 copy-start.1
  28.0 0.7 copy-done.1
  28.7 3.7 %stage.1 = (bf16[4,512,512]{2,1,0:T(8,128)(2,1)S(1)}, bf16[2,512,512]{2,1,0:T(8,128)(2,1)S(1)}, f32[4,8,512]{2,1,0:T(8,128)S(1)}, f32[16,16]{1,0:T(8,128)S(1)}, ...) custom-call(bf16[4,512,512]{2,1,0:T(8,128)(2,1)} %key_hbm.1, bf16[4,512,512]{2,1,0:T(8,128)(2,1)} %value_hbm.2, ...), custom_call_target="tpu_custom_call" | custom-call | flops 500000000 | bytes 8500000 | tf_op jit(solution)/shard_map/stage/pallas_call | solution.py:539
  32.4 6.2 %all-to-all-done.1.got_ref = bf16[32,32,128]{2,1,0:T(8,128)(2,1)S(1)} async-done(((bf16[32,32,128]{2,1,0:T(8,128)(2,1)}), bf16[32,32,128]{2,1,0:T(8,128)(2,1)S(1)}, u32[]{:S(2)}, u32[]{:S(2)}) %all-to-all-start.1) | async-done | bytes 262176 | tf_op jit(solution)/shard_map/all_to_all | solution.py:455
  38.6 0.0 copy-start
  38.6 2.0 %attend.1 = (f32[288,128]{1,0:T(8,128)S(1)}, f32[16,128]{1,0:T(8,128)S(1)}, bf16[16,128]{1,0:T(8,128)(2,1)S(1)}) custom-call(f32[8,128]{1,0:T(8,128)S(1)} %get-tuple-element.32.consts_ref, f32[8,128]{1,0:T(8,128)S(1)} %get-tuple-element.35.inverse_ref, f32[1,128]{1,0:T(1,128)S(1)} %get-tuple-element.37.row_ref, f32[16,16]{1,0:T(8,128)S(1)} %get-tuple-element.41.bias_ref, ...), custom_call_target="tpu_custom_call" | custom-call | flops 600000000 | bytes 4500000 | tf_op jit(solution)/shard_map/attend/pallas_call | solution.py:560
  40.5 13.3 %all_to_all.21 = f32[32,1,1152]{2,1,0:T(1,128)S(1)} all-to-all(f32[32,1,1152]{2,1,0:T(1,128)S(1)} %bitcast.18), channel_id=1, replica_groups=mesh['dp'=4,'kv'=32,'tp'=2] {'kv'}, dimensions={0} | all-to-all | bytes 294912 | tf_op jit(solution)/shard_map/all_to_all | solution.py:455
  53.9 0.4 merge.1
  54.2 13.0 %all_to_all.22.got_ref = bf16[32,24,128]{2,1,0:T(8,128)(2,1)S(1)} all-to-all(bf16[32,24,128]{2,1,0:T(8,128)(2,1)S(1)} %merge.1), channel_id=1, replica_groups=mesh['dp'=4,'kv'=32,'tp'=2] {'kv'}, dimensions={0} | all-to-all | bytes 393216 | tf_op jit(solution)/shard_map/all_to_all | solution.py:455
  67.2 0.0 copy-done
  67.2 0.2 out.1
  67.4 5.7 %collective-permute-start = (bf16[64,64]{1,0:T(8,128)(2,1)S(1)}, bf16[64,64]{1,0:T(8,128)(2,1)S(1)}, u32[]{:S(2)}, u32[]{:S(2)}) collective-permute-start(bf16[64,64]{1,0:T(8,128)(2,1)S(1)} %out.1), channel_id=1, source_target_pairs={{0,1},{1,0},{2,3},{3,2},{4,5},{5,4},{6,7},{7,6},{8,9},{9,8},{10,11... | collective-permute-start | bytes 24584 | tf_op jit(solution)/shard_map/ppermute | solution.py:598
  73.1 0.9 %write.1 = (bf16[4,512,512]{2,1,0:T(8,128)(2,1)}, bf16[4,512,512]{2,1,0:T(8,128)(2,1)}, f32[4,8,16]{2,1,0:T(8,128)}) custom-call(f32[8,128]{1,0:T(8,128)S(1)} %get-tuple-element.32.consts_ref, f32[288,128]{1,0:T(8,128)S(1)} %bitcast.16, bf16[32,24,128]{2,1,0:T(8,128)(2,1)S(1)} %all_to_all.22.got_ref, ...), custom_call_target="tpu_custom_call", output_to_operand_aliasing={{0}: (5, {}), {1}: (6, {})} | custom-call | flops 60000000 | bytes 1000000 | tf_op jit(solution)/shard_map/write/pallas_call | solution.py:600
  74.0 0.0 collective-permute-done
  74.1 0.6 add_convert_fusion
Async XLA Ops:
  24.1 14.4 %all-to-all-start.1 = ((bf16[32,32,128]{2,1,0:T(8,128)(2,1)}), bf16[32,32,128]{2,1,0:T(8,128)(2,1)S(1)}, u32[]{:S(2)}, u32[]{:S(2)}) async-start(bf16[32,32,128]{2,1,0:T(8,128)(2,1)} %get-tuple-element.42), calls=%async_computation.1 | async-start | bytes 524288 | tf_op jit(solution)/shard_map/all_to_all | solution.py:455
  28.0 0.7 copy-start.1
  38.6 28.7 %copy-start = (bf16[512,64]{0,1:T(8,128)(2,1)S(1)}, bf16[512,64]{0,1:T(8,128)(2,1)}, u32[]{:S(2)}) copy-start(bf16[512,64]{0,1:T(8,128)(2,1)} %param.27) | copy-start | bytes 196612
  67.4 6.6 %collective-permute-start = (bf16[64,64]{1,0:T(8,128)(2,1)S(1)}, bf16[64,64]{1,0:T(8,128)(2,1)S(1)}, u32[]{:S(2)}, u32[]{:S(2)}) collective-permute-start(bf16[64,64]{1,0:T(8,128)(2,1)S(1)} %out.1), channel_id=1, source_target_pairs={{0,1},{1,0},{2,3},{3,2},{4,5},{5,4},{6,7},{7,6},{8,9},{9,8},{10,11... | collective-permute-start | bytes 24584 | tf_op jit(solution)/shard_map/ppermute | solution.py:598
